TPU v7x, 256 devices: a whole 4x4x8 slice. The times are simulated.
256 devices in a mesh: ep: 64 (over z, y, core), tp: 4 (over x).
Axes of the slice: x: 4, y: 4, z: 8, core: 2. Of those that a mesh axis runs over, the one named last changes fastest.
Arguments:
- tokens: bfloat16 [3072, 2048], P('ep'), may hold values from -6 to 6
- out_grad: bfloat16 [3072, 2048], P('ep'), may hold values from -4 to 4
- expert_ids: int32 [3072, 4], P('ep'), may hold values from 0 to 63, all different within a row; in each aligned block of 48 rows (0 to 47, 48 to 95, ...) at most 8 rows name the same one
- router_weight: bfloat16 [2048, 64], replicated, may hold values from -0.125 to 0.125
- w_gate: bfloat16 [64, 2048, 1536], P('ep', None, 'tp'), may hold values from -0.125 to 0.125
- w_up: bfloat16 [64, 2048, 1536], P('ep', None, 'tp'), may hold values from -0.125 to 0.125
- w_down: bfloat16 [64, 1536, 2048], P('ep', 'tp'), may hold values from -0.15625 to 0.15625
Outputs:
- token_grad: bfloat16 [3072, 2048], P('ep', 'tp')
- router_grad: float32 [2048, 64], P('tp', 'ep')
- w_gate_grad: bfloat16 [64, 2048, 1536], P('ep', None, 'tp')
- w_up_grad: bfloat16 [64, 2048, 1536], P('ep', None, 'tp')
- w_down_grad: bfloat16 [64, 1536, 2048], P('ep', 'tp')
Inputs may be any that keep to these rules, and one draw needn't show every extreme that they name: `expert_ids`: each row names 4 different experts; among the rows of one device no expert is named more than 8 times, and in some devices' rows one expert is named exactly 8 times.
All inputs are finite; a program needn't handle non-finite values.
Results may differ from a plain program's by a relative error of at most 0.0058.
Values may be sent and summed in bfloat16 or wider, within the bound.
A program may use at most 128 MiB of HBM per device.

v0:
```python
import jax
import jax.numpy as jnp
from jax import lax
from jax.sharding import PartitionSpec as P


def side_by_side(arrays, axis, split_dim, concat_dim, along):
    both = jnp.concatenate(arrays, axis=along)
    out, at, gathered = (
        lax.all_to_all(both, axis, split_axis=split_dim, concat_axis=concat_dim, tiled=True),
        0,
        [],
    )
    for a in arrays:
        gathered.append(lax.slice_in_dim(out, at, at + a.shape[along], axis=along))
        at += a.shape[along]
    return tuple(gathered)


def side_by_side_2(arrays, axis, dim, along):
    both = jnp.concatenate(arrays, axis=along)
    out, at, gathered = (lax.all_gather(both, axis, axis=dim, tiled=True), 0, [])
    for a in arrays:
        gathered.append(lax.slice_in_dim(out, at, at + a.shape[along], axis=along))
        at += a.shape[along]
    return tuple(gathered)


def laid_out(blocks, dim):
    dims = list(blocks.shape[1:])
    dims[dim] *= blocks.shape[0]
    return jnp.moveaxis(blocks, 0, dim).reshape(dims)


def from_everyone(value, axis):
    copies = jnp.broadcast_to(value, (lax.axis_size(axis), *value.shape))
    return lax.all_to_all(copies, axis, split_axis=0, concat_axis=0, tiled=True)


def collect(value, axis, dim):
    return laid_out(from_everyone(value, axis), dim)


def split_up(value, dim, devices):
    before, after = (value.shape[:dim], value.shape[dim + 1 :])
    return jnp.moveaxis(value.reshape(*before, devices, -1, *after), dim, 0)


def summed_on_arrival(value, axis, dim):
    devices = lax.axis_size(axis)
    blocks = lax.all_to_all(split_up(value, dim, devices), axis, 0, 0, tiled=True)
    return jnp.sum(blocks.astype(jnp.float32), axis=0)


def side_by_side_3(arrays, axis, split_dim, concat_dim, along):
    columns = [a.reshape(*a.shape[:along], -1) for a in arrays]
    both = jnp.concatenate(columns, axis=along)
    out, at, gathered = (
        lax.all_to_all(both, axis, split_axis=split_dim, concat_axis=concat_dim, tiled=True),
        0,
        [],
    )
    for a, column in zip(arrays, columns):
        piece = out[..., at : at + column.shape[along]]
        gathered.append(piece.reshape(*piece.shape[:along], *a.shape[along:]))
        at += column.shape[along]
    return tuple(gathered)


def taken_together(value, axis):
    return from_everyone(value, axis).sum(axis=0)


def sum_at_owner(value, axis, dim):
    blocks = split_up(value, dim, lax.axis_size(axis))
    arrived = lax.all_to_all(blocks, axis, split_axis=0, concat_axis=0, tiled=True)
    return arrived.sum(axis=0)


def activation_parts(gate_pre, up_pre):
    glu = jnp.minimum(gate_pre, 7.0)
    linear = jnp.clip(up_pre, -7.0, 7.0)
    sigma = jax.nn.sigmoid(1.702 * glu)
    act_value = glu * sigma
    hidden = (linear + 1.0) * act_value
    slope = (linear + 1.0) * (sigma + 1.702 * glu * sigma * (1.0 - sigma))
    slope = jnp.where(gate_pre < 7.0, slope, 0.0)
    up_slope = jnp.where((up_pre > -7.0) & (up_pre < 7.0), act_value, 0.0)
    return (hidden, slope, up_slope)


def contract_last(left, right):
    return lax.dot_general(
        left, right, (((1,), (1,)), ((), ())), preferred_element_type=jnp.float32
    )


def contract_first(left, right):
    return lax.dot_general(
        left, right, (((0,), (0,)), ((), ())), preferred_element_type=jnp.float32
    )


def per_device(tokens, out_grad, expert_ids, router_weight, w_gate, w_up, w_down):
    tok_dev, model_width = tokens.shape
    top_count = expert_ids.shape[1]
    expert_count = router_weight.shape[1]
    peer_count = lax.axis_size("ep")
    tp_count = lax.axis_size("tp")
    capacity = min(
        tok_dev,
        tp_count * max(1, (2 * tok_dev * top_count // expert_count + tp_count - 1) // tp_count),
    )
    feature_part = model_width // tp_count
    logits = jnp.dot(tokens, router_weight, preferred_element_type=jnp.float32)
    chosen = jnp.take_along_axis(logits, expert_ids, axis=1)
    gate_values = jax.nn.softmax(chosen, axis=-1)
    flat_ids = expert_ids.reshape(-1)
    one_hot = (flat_ids[:, None] == jnp.arange(expert_count, dtype=jnp.int32)[None, :]).astype(
        jnp.int32
    )
    slot_rank = jnp.sum((jnp.cumsum(one_hot, axis=0) - one_hot) * one_hot, axis=1)
    slot_index = flat_ids * capacity + slot_rank
    flat_tok = jnp.arange(tok_dev * top_count, dtype=jnp.int32) // top_count
    buffer_rows = expert_count * capacity
    sent_tokens = (
        jnp.zeros((buffer_rows, model_width), jnp.bfloat16).at[slot_index].set(tokens[flat_tok])
    )
    sent_grads = (
        jnp.zeros((buffer_rows, model_width), jnp.bfloat16).at[slot_index].set(out_grad[flat_tok])
    )
    sent_gates = jnp.zeros((buffer_rows,), jnp.float32).at[slot_index].set(gate_values.reshape(-1))
    slot_tokens = sent_tokens.reshape(expert_count, capacity, model_width)
    slot_grads = sent_grads.reshape(expert_count, capacity, model_width)
    slot_gates = sent_gates.reshape(expert_count, capacity)
    slot_share = capacity // tp_count
    share_start = lax.axis_index("tp") * slot_share
    part_tokens = lax.dynamic_slice_in_dim(slot_tokens, share_start, slot_share, 1)
    part_grads = lax.dynamic_slice_in_dim(slot_grads, share_start, slot_share, 1)
    part_gates = lax.dynamic_slice_in_dim(slot_gates, share_start, slot_share, 1)
    got_tokens, got_grads = side_by_side((part_tokens, part_grads), "ep", 0, 0, 1)
    got_gates = lax.all_to_all(part_gates, "ep", split_axis=0, concat_axis=0, tiled=True)
    recv_tokens, recv_grads = side_by_side_2((got_tokens, got_grads), "tp", 1, 0)
    recv_gates = collect(got_gates, "tp", 1)
    slot_count = peer_count * capacity
    inputs_rows = recv_tokens.reshape(slot_count, model_width)
    grad_rows = recv_grads.reshape(slot_count, model_width)
    weight_rows = recv_gates.reshape(slot_count)
    gate_mat = w_gate[0]
    up_mat = w_up[0]
    down_mat = w_down[0]
    gate_pre = jnp.dot(inputs_rows, gate_mat, preferred_element_type=jnp.float32)
    up_pre = jnp.dot(inputs_rows, up_mat, preferred_element_type=jnp.float32)
    hidden, slope, up_slope = activation_parts(gate_pre, up_pre)
    back_proj = contract_last(grad_rows, down_mat)
    gate_score = jnp.sum(hidden * back_proj, axis=1)
    d_hidden = weight_rows[:, None] * back_proj
    d_gate_pre = (d_hidden * slope).astype(jnp.bfloat16)
    d_up_pre = (d_hidden * up_slope).astype(jnp.bfloat16)
    weighted = (weight_rows[:, None] * hidden).astype(jnp.bfloat16)
    w_down_grad = contract_first(weighted, grad_rows).astype(jnp.bfloat16)[None]
    w_gate_grad = contract_first(inputs_rows, d_gate_pre).astype(jnp.bfloat16)[None]
    w_up_grad = contract_first(inputs_rows, d_up_pre).astype(jnp.bfloat16)[None]
    summed_part = summed_on_arrival(
        (contract_last(gate_mat, d_gate_pre) + contract_last(up_mat, d_up_pre)).astype(
            jnp.bfloat16
        ),
        "tp",
        0,
    )
    returned = summed_part.T.reshape(peer_count, capacity, feature_part)
    home_grads, home_scores = side_by_side_3(
        (returned, gate_score.reshape(peer_count, capacity)), "ep", 0, 0, 2
    )
    picked = home_grads.reshape(buffer_rows, feature_part)[slot_index]
    expert_part = jnp.sum(picked.reshape(tok_dev, top_count, feature_part), axis=1)
    local_scores = home_scores.reshape(buffer_rows)[slot_index].reshape(tok_dev, top_count)
    total_scores = taken_together(local_scores, "tp")
    d_chosen = gate_values * (
        total_scores - jnp.sum(gate_values * total_scores, axis=-1, keepdims=True)
    )
    expert_hot = (
        expert_ids[:, :, None] == jnp.arange(expert_count, dtype=jnp.int32)[None, None, :]
    ).astype(jnp.float32)
    d_logits = jnp.sum(d_chosen[:, :, None] * expert_hot, axis=1)
    column = lax.axis_index("tp") * feature_part
    local_tokens = lax.dynamic_slice_in_dim(tokens, column, feature_part, 1).astype(jnp.float32)
    router_term = jnp.dot(local_tokens.T, d_logits, precision=lax.Precision.HIGHEST)
    router_grad = sum_at_owner(router_term, "ep", 1)
    router_rows = lax.dynamic_slice_in_dim(router_weight, column, feature_part, 0).astype(
        jnp.float32
    )
    router_part = jnp.dot(d_logits, router_rows.T, precision=lax.Precision.HIGHEST)
    token_grad = (expert_part + router_part).astype(jnp.bfloat16)
    return (token_grad, router_grad, w_gate_grad, w_up_grad, w_down_grad)


def solution(mesh):
    in_specs = (
        P("ep", None),
        P("ep", None),
        P("ep", None),
        P(),
        P("ep", None, "tp"),
        P("ep", None, "tp"),
        P("ep", "tp", None),
    )
    out_specs = (
        P("ep", "tp"),
        P("tp", "ep"),
        P("ep", None, "tp"),
        P("ep", None, "tp"),
        P("ep", "tp", None),
    )
    return jax.shard_map(
        per_device, mesh=mesh, in_specs=in_specs, out_specs=out_specs, check_vma=False
    )
```

profile of v0, /device:TPU:1, one launch (start us, length us, event | category | flops | bytes accessed | tf_op | source)
XLA Modules:
  0.0 254.1 jit_solution(215335838511083896)
XLA Ops:
  7.2 0.9 copy.101
  8.1 0.7 broadcast_multiply_fusion
  8.8 0.1 eq.35
  8.9 0.6 reduce-window.6
  9.5 0.2 slice_reduce_fusion.1
  10.0 0.1 mul.87
  10.1 6.4 %scatter_custom_fusion.1 = bf16[512,2048]{1,0:T(8,128)(2,1)} fusion(s32[192]{0:T(256)S(1)} %bitcast.99, bf16[]{:T(256)} %constant.65.clone.1, bf16[48,2048]{1,0:T(8,128)(2,1)} %param.7, s32[1024]{0:T(1024)S(1)} %pad_clamp_fusion.1), kind=kCustom, calls=%fused_computation.37 | custom fusion | bytes 2097664 | tf_op jit(solution)/shard_map/scatter | solution.py:127
  16.6 6.5 %scatter_custom_fusion.2 = bf16[512,2048]{1,0:T(8,128)(2,1)} fusion(s32[192]{0:T(256)S(1)} %bitcast.100, bf16[]{:T(256)} %constant.65.clone.1, bf16[48,2048]{1,0:T(8,128)(2,1)} %param.8, s32[1024]{0:T(1024)S(1)} %pad_clamp_fusion.1), kind=kCustom, calls=%fused_computation.35 | custom fusion | bytes 2097664 | tf_op jit(solution)/shard_map/scatter | solution.py:130
  23.0 2.1 constant_dynamic-slice_fusion.1
  25.2 2.1 constant_dynamic-slice_fusion
  27.3 1.1 pad_maximum_fusion.1
  28.4 41.1 %all_to_all.42 = bf16[64,4,2048]{2,1,0:T(4,128)(2,1)S(1)} all-to-all(bf16[64,4,2048]{2,1,0:T(4,128)(2,1)S(1)} %pad_maximum_fusion.1), channel_id=1, replica_groups=mesh['ep'=64,'tp'=4] {'ep'}, dimensions={0} | all-to-all | bytes 2097152 | tf_op jit(solution)/shard_map/all_to_all | solution.py:10
  69.5 0.7 fusion.37
  70.3 1.4 pad_maximum_fusion.2
  71.7 1.3 copy.111
  73.1 0.1 reshape.227
  73.3 0.2 fusion.38
  73.5 1.6 gather_fusion.2
  75.1 0.1 reshape.230
  75.4 0.1 reshape.237
  75.6 0.4 copy-done.10
  75.9 1.2 scatter_custom_fusion
  77.3 15.5 %all_to_all.43 = f32[64,1,2]{2,1,0:T(1,128)S(1)} all-to-all(f32[64,1,2]{2,1,0:T(1,128)S(1)} %bitcast.96), channel_id=1, replica_groups=mesh['ep'=64,'tp'=4] {'ep'}, dimensions={0} | all-to-all | bytes 1024 | tf_op jit(solution)/shard_map/all_to_all | solution.py:142
  92.9 8.2 %all_to_all.44 = f32[4,1,128]{2,1,0:T(1,128)S(1)} all-to-all(f32[4,1,128]{2,1,0:T(1,128)S(1)} %reshape.278), channel_id=1, replica_groups=mesh['ep'=64,'tp'=4] {'tp'}, dimensions={0} | all-to-all | bytes 4096 | tf_op jit(solution)/shard_map/all_to_all | solution.py:37
  101.1 0.6 broadcast.245
  101.7 0.6 reduce.5
  102.4 0.1 copy.110
  102.5 0.2 mul.90
  102.7 17.9 %all-gather.2.cloned.1.call-done = bf16[128,8,2048]{2,0,1:T(8,128)(2,1)} async-done(((bf16[128,2,2048]{2,0,1:T(8,128)(2,1)}), bf16[128,8,2048]{2,0,1:T(8,128)(2,1)}) %all-gather.2.cloned.1.call-update) | async-done | bytes 4194320 | tf_op jit(solution)/shard_map/all_gather | solution.py:22
  120.7 2.7 %fusion.36 = (bf16[64,8,2048]{2,0,1:T(8,128)(2,1)S(1)}, bf16[64,8,2048]{2,0,1:T(8,128)(2,1)S(1)}) fusion(bf16[128,8,2048]{2,0,1:T(8,128)(2,1)} %all-gather.2.cloned.1.call-done), kind=kLoop, calls=%fused_computation.93 | loop fusion | bytes 8388608 | tf_op jit(solution)/shard_map/slice | solution.py:24
  123.4 1.6 fusion.9
  125.1 0.9 copy-done.17
  126.0 1.5 fusion.3
  127.6 3.6 %multiply_convert_fusion.1 = (bf16[512,384]{0,1:T(8,128)(2,1)S(1)}, bf16[512,384]{0,1:T(8,128)(2,1)S(1)}, f32[512]{0:T(512)}, f32[512,384]{0,1:T(8,128)}) fusion(f32[512,384]{0,1:T(8,128)S(1)} %fusion.3, f32[512]{0:T(512)S(1)} %mul.90, f32[512,384]{0,1:T(8,128)S(1)} %fusion.9, bf16[1,2048,384]{2,1,0:T(8,128)(2,1)S(1)} %copy-done, ...), kind=kOutput, calls=%fused_computation.43 | convolution fusion | flops 810614272 | bytes 6819840 | tf_op jit(solution)/shard_map/dot_general | solution.py:153
  131.2 1.3 fusion.7
  132.5 1.3 add_convert_fusion
  133.8 1.5 copy.138
  135.3 4.6 %all-to-all-start.3 = ((bf16[4,512,512]{1,2,0:T(8,128)(2,1)}), bf16[4,512,512]{1,2,0:T(8,128)(2,1)}, u32[]{:S(2)}, u32[]{:S(2)}) async-start(bf16[4,512,512]{1,2,0:T(8,128)(2,1)} %bitcast.91), calls=%async_computation.3 | async-start | bytes 4194304 | tf_op jit(solution)/shard_map/all_to_all | solution.py:51
  139.9 0.2 reshape_reshape.8
  140.1 25.4 %all-to-all-done.3 = bf16[4,512,512]{1,2,0:T(8,128)(2,1)} async-done(((bf16[4,512,512]{1,2,0:T(8,128)(2,1)}), bf16[4,512,512]{1,2,0:T(8,128)(2,1)}, u32[]{:S(2)}, u32[]{:S(2)}) %all-to-all-start.3) | async-done | bytes 2097184 | tf_op jit(solution)/shard_map/all_to_all | solution.py:51
  165.6 2.0 convert_reduce_fusion
  167.6 1.2 pad_maximum_fusion
  168.8 11.7 %all-to-all-start.4 = ((f32[64,8,513]{2,1,0:T(8,128)}), f32[64,8,513]{2,1,0:T(8,128)S(1)}, u32[]{:S(2)}, u32[]{:S(2)}) async-start(f32[64,8,513]{2,1,0:T(8,128)} %pad_maximum_fusion), calls=%async_computation.4 | async-start | bytes 2621440 | tf_op jit(solution)/shard_map/all_to_all | solution.py:59
  180.6 4.6 %fusion.1 = bf16[1,2048,384]{2,1,0:T(8,128)(2,1)} fusion(bf16[512,384]{0,1:T(8,128)(2,1)} %copy-done.7, bf16[64,8,2048]{2,0,1:T(8,128)(2,1)} %copy-done.2), kind=kOutput, calls=%fused_computation.14 | convolution fusion | flops 806092800 | bytes 4063232 | tf_op jit(solution)/shard_map/dot_general | solution.py:99
  185.1 3.0 %fusion.2 = bf16[1,384,2048]{2,1,0:T(8,128)(2,1)} fusion(bf16[64,8,2048]{2,0,1:T(8,128)(2,1)S(1)} %copy-done.4, f32[512]{0:T(512)S(1)} %copy-done.15, f32[512,384]{0,1:T(8,128)S(1)} %copy-done.20, f32[512,384]{0,1:T(8,128)S(1)} %copy-done.19), kind=kOutput, calls=%fused_computation.15 | convolution fusion | flops 808255488 | bytes 5244928 | tf_op jit(solution)/shard_map/dot_general | solution.py:99
  188.1 26.0 %all-to-all-done.4 = f32[64,8,513]{2,1,0:T(8,128)S(1)} async-done(((f32[64,8,513]{2,1,0:T(8,128)}), f32[64,8,513]{2,1,0:T(8,128)S(1)}, u32[]{:S(2)}, u32[]{:S(2)}) %all-to-all-start.4) | async-done | bytes 1050656 | tf_op jit(solution)/shard_map/all_to_all | solution.py:59
  214.1 1.1 copy-done.1
  215.2 0.1 slice_reduce_fusion
  215.4 1.6 gather_fusion.1
  217.2 0.7 reshape.280
  217.9 3.2 %all-to-all-start.5 = ((f32[4,1,192]{2,1,0:T(1,128)}), f32[4,1,192]{2,1,0:T(1,128)S(1)}, u32[]{:S(2)}, u32[]{:S(2)}) async-start(f32[4,1,192]{2,1,0:T(1,128)} %reshape.280), calls=%async_computation.5 | async-start | bytes 8192 | tf_op jit(solution)/shard_map/all_to_all | solution.py:37
  221.2 4.4 %fusion = bf16[1,2048,384]{2,1,0:T(8,128)(2,1)} fusion(bf16[512,384]{0,1:T(8,128)(2,1)S(1)} %get-tuple-element.10, bf16[64,8,2048]{2,0,1:T(8,128)(2,1)} %copy-done.2), kind=kOutput, calls=%fused_computation.13 | convolution fusion | flops 806092800 | bytes 4063232 | tf_op jit(solution)/shard_map/dot_general | solution.py:99
  225.5 0.6 reduce.6
  226.3 0.1 select_reduce_fusion
  226.5 1.1 convolution_bitcast_fusion
  227.5 0.8 copy.117
  228.3 7.2 %all-to-all-start.6 = ((f32[64,512,1]{1,2,0:T(1,128)}), f32[64,512,1]{1,2,0:T(1,128)S(1)}, u32[]{:S(2)}, u32[]{:S(2)}) async-start(f32[64,512,1]{1,2,0:T(1,128)} %copy.117), calls=%async_computation.6 | async-start | bytes 262144 | tf_op jit(solution)/shard_map/all_to_all | solution.py:76
  235.5 1.3 slice_bitcast_fusion
  236.8 0.9 gather_fusion
  237.7 0.1 reshape.191
  237.8 0.2 reduce_sum.90
  238.0 1.6 fusion.12
  239.7 6.9 %all-to-all-done.6 = f32[64,512,1]{1,2,0:T(1,128)S(1)} async-done(((f32[64,512,1]{1,2,0:T(1,128)}), f32[64,512,1]{1,2,0:T(1,128)S(1)}, u32[]{:S(2)}, u32[]{:S(2)}) %all-to-all-start.6) | async-done | bytes 131104 | tf_op jit(solution)/shard_map/all_to_all | solution.py:76
  246.6 0.7 reduce_sum.94
  (74 shorter events, 1.6 us)
Async XLA Ops:
  7.2 120.4 %copy-start = (bf16[1,2048,384]{2,1,0:T(8,128)(2,1)S(1)}, bf16[1,2048,384]{2,1,0:T(8,128)(2,1)}, u32[]{:S(2)}) copy-start(bf16[1,2048,384]{2,1,0:T(8,128)(2,1)} %param.12) | copy-start | bytes 4718596
  7.2 113.5 %all-gather.2.cloned.1.call-start = ((), (), s32[]{:S(2)}) async-start(), calls=%async_computation.7 | async-start | bytes 5242880 | tf_op jit(solution)/shard_map/all_gather | solution.py:22
  10.1 65.4 %copy-start.12 = (s32[192,1]{0,1:T(1,128)}, s32[192,1]{0,1:T(1,128)S(1)}, u32[]{:S(2)}) copy-start(s32[192,1]{0,1:T(1,128)S(1)} %get-tuple-element.16) | copy-start | bytes 2308
  71.6 1.4 copy-start.9
  71.6 1.6 copy-start.6
  71.7 1.6 copy-start.8
  75.3 0.6 copy-start.10
  102.7 24.8 %copy-start.14 = (f32[512]{0:T(512)}, f32[512]{0:T(512)S(1)}, u32[]{:S(2)}) copy-start(f32[512]{0:T(512)S(1)} %mul.90) | copy-start | bytes 6148
  102.7 20.7 %copy-start.5 = (bf16[1,2048,384]{2,1,0:T(8,128)(2,1)S(1)}, bf16[1,2048,384]{2,1,0:T(8,128)(2,1)}, u32[]{:S(2)}) copy-start(bf16[1,2048,384]{2,1,0:T(8,128)(2,1)} %param.11) | copy-start | bytes 4718596
  123.4 1.7 copy-start.3
  123.4 4.1 %copy-start.2 = (bf16[64,8,2048]{2,0,1:T(8,128)(2,1)}, bf16[64,8,2048]{2,0,1:T(8,128)(2,1)S(1)}, u32[]{:S(2)}) copy-start(bf16[64,8,2048]{2,0,1:T(8,128)(2,1)S(1)} %get-tuple-element.7) | copy-start | bytes 6291460
  123.4 2.6 %copy-start.17 = (bf16[1,384,2048]{2,1,0:T(8,128)(2,1)S(1)}, bf16[1,384,2048]{2,1,0:T(8,128)(2,1)}, u32[]{:S(2)}) copy-start(bf16[1,384,2048]{2,1,0:T(8,128)(2,1)} %param.13) | copy-start | bytes 4718596
  125.1 2.5 copy-start.18
  131.2 1.3 copy-start.7
  135.3 4.6 %copy-start.16 = (f32[512]{0:T(512)S(1)}, f32[512]{0:T(512)}, u32[]{:S(2)}) copy-start(f32[512]{0:T(512)} %get-tuple-element.11) | copy-start | bytes 6148
  135.3 30.2 %all-to-all-start.3 = ((bf16[4,512,512]{1,2,0:T(8,128)(2,1)}), bf16[4,512,512]{1,2,0:T(8,128)(2,1)}, u32[]{:S(2)}, u32[]{:S(2)}) async-start(bf16[4,512,512]{1,2,0:T(8,128)(2,1)} %bitcast.91), calls=%async_computation.3 | async-start | bytes 4194304 | tf_op jit(solution)/shard_map/all_to_all | solution.py:51
  167.6 12.9 %copy-start.13 = (s32[192,1]{0,1:T(1,128)S(1)}, s32[192,1]{0,1:T(1,128)}, u32[]{:S(2)}) copy-start(s32[192,1]{0,1:T(1,128)} %copy-done.12) | copy-start | bytes 2308
  168.8 45.3 %all-to-all-start.4 = ((f32[64,8,513]{2,1,0:T(8,128)}), f32[64,8,513]{2,1,0:T(8,128)S(1)}, u32[]{:S(2)}, u32[]{:S(2)}) async-start(f32[64,8,513]{2,1,0:T(8,128)} %pad_maximum_fusion), calls=%async_computation.4 | async-start | bytes 2621440 | tf_op jit(solution)/shard_map/all_to_all | solution.py:59
  180.5 4.6 %copy-start.4 = (bf16[64,8,2048]{2,0,1:T(8,128)(2,1)S(1)}, bf16[64,8,2048]{2,0,1:T(8,128)(2,1)}, u32[]{:S(2)}) copy-start(bf16[64,8,2048]{2,0,1:T(8,128)(2,1)} %copy-done.3) | copy-start | bytes 6291460
  180.5 4.6 %copy-start.15 = (f32[512]{0:T(512)S(1)}, f32[512]{0:T(512)}, u32[]{:S(2)}) copy-start(f32[512]{0:T(512)} %copy-done.14) | copy-start | bytes 6148
  180.5 4.6 %copy-start.19 = (f32[512,384]{0,1:T(8,128)S(1)}, f32[512,384]{0,1:T(8,128)}, u32[]{:S(2)}) copy-start(f32[512,384]{0,1:T(8,128)} %copy-done.18) | copy-start | bytes 2359300
  180.5 4.6 %copy-start.20 = (f32[512,384]{0,1:T(8,128)S(1)}, f32[512,384]{0,1:T(8,128)}, u32[]{:S(2)}) copy-start(f32[512,384]{0,1:T(8,128)} %get-tuple-element.14) | copy-start | bytes 2359300
  214.1 1.1 copy-start.1
  217.9 7.6 %all-to-all-start.5 = ((f32[4,1,192]{2,1,0:T(1,128)}), f32[4,1,192]{2,1,0:T(1,128)S(1)}, u32[]{:S(2)}, u32[]{:S(2)}) async-start(f32[4,1,192]{2,1,0:T(1,128)} %reshape.280), calls=%async_computation.5 | async-start | bytes 8192 | tf_op jit(solution)/shard_map/all_to_all | solution.py:37
  221.2 5.1 %copy-start.11 = (f32[48]{0:T(128)S(1)}, f32[48]{0:T(128)}, u32[]{:S(2)}) copy-start(f32[48]{0:T(128)} %copy-done.10) | copy-start | bytes 580
  228.3 18.3 %all-to-all-start.6 = ((f32[64,512,1]{1,2,0:T(1,128)}), f32[64,512,1]{1,2,0:T(1,128)S(1)}, u32[]{:S(2)}, u32[]{:S(2)}) async-start(f32[64,512,1]{1,2,0:T(1,128)} %copy.117), calls=%async_computation.6 | async-start | bytes 262144 | tf_op jit(solution)/shard_map/all_to_all | solution.py:76
Sparse Core Ops, SparseCore 0:
  73.1 47.4 all-gather.1
where the time goes:
time: 255 us; the launch traced here: 254 us
  waiting for transfers between devices  76.3 us (30%)
  blocking collectives  64.8 us (25%)
  local copies, waits for them, and re-layouts  38 us (15%)
  starting transfers between devices  26.8 us (11%)
  matrix products  24.2 us (9%)
  between operations  14.6 us (6%)
  other arithmetic  9.56 us (4%)
    all_to_all x1, blocking collectives, side_by_side(): lax.all_to_all(both, axis, split_axis=split_dim, concat_axis=concat_dim,...  41.1 us
    all_to_all x1, waiting for transfers between devices, side_by_side_3(): lax.all_to_all(both, axis, split_axis=split_dim, concat_axis=concat_dim,...  26 us
    all_to_all x1, waiting for transfers between devices, summed_on_arrival(): lax.all_to_all(split_up(value, dim, devices), axis, 0, 0, tiled=True)  25.4 us
    all_gather x1, waiting for transfers between devices, side_by_side_2(): lax.all_gather(both, axis, axis=dim, tiled=True)  17.9 us
    all_to_all x1, blocking collectives, per_device(): lax.all_to_all(part_gates, 'ep', split_axis=0, concat_axis=0, tiled=True)  15.5 us
    scatter x2, local copies, waits for them, and re-layouts, per_device(): jnp.zeros((buffer_rows, model_width), jnp.bfloat16).at[slot_index]  12.9 us
    dot_general x3, matrix products, contract_first(): lax.dot_general(left, right, (((0,), (0,)), ((), ())), preferred_element_...  11.9 us
    all_to_all x1, starting transfers between devices, side_by_side_3(): lax.all_to_all(both, axis, split_axis=split_dim, concat_axis=concat_dim,...  11.7 us
  transfers between devices with their start and end apart: 5, of which 4 were waited for; matrix products, arithmetic and copies ran while one was open for 9% of the time, Pallas kernels for 0%

commit v1 on v0

v1 whole, which is shorter than its diff:
```python
import functools

import jax
import jax.numpy as jnp
from jax import lax
from jax.experimental import pallas as pl
from jax.experimental.pallas import tpu as pltpu
from jax.sharding import PartitionSpec as P

MESH = pl.DeviceIdType.MESH
F32 = jnp.float32
BF16 = jnp.bfloat16
NK = 8
NE = 8
CAP = 8
PAIR_OF = (0, 2, 1, 4, 3, 6, 5, 7)


def dot_last(a, b):
    return lax.dot_general(a, b, (((1,), (1,)), ((), ())), preferred_element_type=F32)


def dot_first(a, b):
    return lax.dot_general(a, b, (((0,), (0,)), ((), ())), preferred_element_type=F32)


def dot(a, b):
    return jnp.dot(a, b, preferred_element_type=F32)


def step_kernel(
    tok_hbm,
    grad_hbm,
    ids_ref,
    rw_ref,
    wg_hbm,
    wu_hbm,
    wd_hbm,
    tg_ref,
    rg_ref,
    gg_hbm,
    ug_hbm,
    dg_hbm,
    tokv,
    wg,
    wu,
    wd,
    zbuf,
    square,
    info,
    infoz,
    infoe,
    einfo,
    pbuf,
    ysend,
    buf,
    dgu,
    wtd,
    dxq,
    r1,
    acc,
    s2,
    r2,
    yret,
    yrr,
    wsend,
    wrecv,
    sx,
    sy,
    syr,
    szs,
    smat,
    dmat,
    dz,
    dys,
    de,
    stage,
    stage2,
    ld,
    zss,
    zrs,
    iss,
    irs,
    ess,
    ers,
    yss,
    yrs,
    xss,
    xrs,
    r1s,
    r1r,
    r2s,
    r2r,
    xcs,
    xcr,
    sys_,
    syr_,
    szs_,
    szr_,
    vss,
    vrs,
    wss,
    wrs,
    dzs_,
    dzr_,
    dys_,
    dyr_,
    outs,
):
    ep = lax.axis_index("ep")
    x = lax.axis_index("tp")
    z = ep // NE
    yc = ep % NE
    par = x % 2
    odd = x % 2
    near_a = x + 1 - 2 * odd
    near_b = (x + 3 + 2 * odd) % 4
    far = (x + 2) % 4
    right = (x + 1) % 4
    left = (x + 3) % 4

    def remote(src, dst, ss, rs, e, t):
        return pltpu.make_async_remote_copy(
            src_ref=src,
            dst_ref=dst,
            send_sem=ss,
            recv_sem=rs,
            device_id={"ep": e, "tp": t},
            device_id_type=MESH,
        )

    def z_of(k):
        h = (k + 1) // 2
        s = 1 - 2 * ((k + 1) % 2)
        return (z + s * h + NK) % NK

    def at_z(zz):
        return zz * NE + yc

    def at_e(j):
        return z * NE + j

    barrier = pltpu.get_barrier_semaphore()
    for d in range(1, NK):
        pl.semaphore_signal(
            barrier, inc=1, device_id={"ep": at_z((z + d) % NK), "tp": x}, device_id_type=MESH
        )
    for d in range(1, NE):
        pl.semaphore_signal(
            barrier, inc=1, device_id={"ep": at_e((yc + d) % NE), "tp": x}, device_id_type=MESH
        )
    for d in range(1, 4):
        pl.semaphore_signal(
            barrier, inc=1, device_id={"ep": ep, "tp": (x + d) % 4}, device_id_type=MESH
        )

    load_tok = pltpu.make_async_copy(tok_hbm, tokv, ld.at[0])
    load_tok.start()

    @pl.when(par == 0)
    def _():
        pltpu.make_async_copy(tok_hbm, zbuf.at[0], ld.at[1]).start()

    @pl.when(par == 1)
    def _():
        pltpu.make_async_copy(grad_hbm, zbuf.at[0], ld.at[1]).start()

    load_g = pltpu.make_async_copy(wg_hbm, wg, ld.at[2])
    load_u = pltpu.make_async_copy(wu_hbm, wu, ld.at[3])
    load_d = pltpu.make_async_copy(wd_hbm, wd, ld.at[4])
    load_g.start()
    load_u.start()
    load_d.start()

    load_tok.wait()
    n_tok = tokv.shape[0]
    n_exp = rw_ref.shape[1]
    logits = dot(tokv[...], rw_ref[...])
    lane_e = lax.broadcasted_iota(jnp.int32, (n_tok, n_exp), 1)
    hit = jnp.zeros((n_tok, n_exp), F32)
    for k in range(ids_ref.shape[1]):
        hit = hit + jnp.where(ids_ref[:, k : k + 1] == lane_e, 1.0, 0.0)
    chosen = hit > 0.0
    top = jnp.max(jnp.where(chosen, logits, -jnp.inf), axis=1, keepdims=True)
    expd = jnp.where(chosen, jnp.exp(jnp.where(chosen, logits - top, 0.0)), 0.0)
    gates = expd / jnp.sum(expd, axis=1, keepdims=True)
    row = lax.broadcasted_iota(jnp.int32, (n_tok, n_tok), 0)
    col = lax.broadcasted_iota(jnp.int32, (n_tok, n_tok), 1)
    earlier = jnp.where(col < row, 1.0, 0.0).astype(BF16)
    rank = dot(earlier, hit.astype(BF16))
    square[...] = jnp.full(square.shape, -1.0, F32)
    square[0:n_tok, 0:n_exp] = jnp.where(chosen, rank, -1.0)
    info[0] = square[...].T[0:n_exp, :]
    square[...] = jnp.zeros(square.shape, F32)
    square[0:n_tok, 0:n_exp] = gates
    info[1] = square[...].T[0:n_exp, :]

    pl.semaphore_wait(barrier, (NK - 1) + (NE - 1) + 3)

    pltpu.make_async_copy(tok_hbm, zbuf.at[0], ld.at[1]).wait()

    def z_copy(k, part=None):
        if part is None:
            src, dst, rs = zbuf.at[k], zbuf.at[k + 2], zrs.at[k + 2]
        else:
            half = zbuf.shape[2] // 2
            cols = pl.ds(part * half, half)
            src, dst, rs = zbuf.at[k, :, cols], zbuf.at[7, :, cols], zrs.at[8 - part]
        s = 1 - 2 * ((k + 1) % 2)
        return remote(src, dst, zss.at[k], rs, at_z((z - s + NK) % NK), x)

    z_left = remote(zbuf.at[0], zbuf.at[1], zss.at[0], zrs.at[1], at_z((z + NK - 1) % NK), x)
    z_right = remote(zbuf.at[0], zbuf.at[2], zss.at[7], zrs.at[2], at_z((z + 1) % NK), x)
    z_left.start()
    z_right.start()

    def info_copy(k):
        zz = z_of(k)
        return remote(
            info.at[:, pl.ds(pl.multiple_of(zz * NE, NE), NE)],
            infoz.at[PAIR_OF[k]],
            iss.at[k],
            irs.at[PAIR_OF[k]],
            at_z(zz),
            x,
        )

    for k in range(1, NK):
        info_copy(k).start()
    own = pl.ds(pl.multiple_of(z * NE, NE), NE)
    infoz[0, 0] = info[0, own, :]
    infoz[0, 1] = info[1, own, :]

    def info_wait(k):
        remote(infoz.at[k], infoz.at[k], iss.at[k], irs.at[k], ep, x).wait_recv()

    def y_copy(k, d):
        j = (yc + d) % NE
        return remote(
            ysend.at[k, j], buf.at[par, k * NE + yc], yss.at[k, d], yrs.at[k, d], at_e(j), x
        )

    def y_wait(k, d):
        j = (yc + NE - d) % NE
        remote(
            ysend.at[k, 0], buf.at[par, k * NE + j], yss.at[k, d], yrs.at[k, d], ep, x
        ).wait_recv()

    def z_wait(k):
        @pl.when((k >= 1) & (k <= 6))
        def _():
            remote(zbuf.at[k], zbuf.at[k], zss.at[0], zrs.at[k], ep, x).wait_recv()

        @pl.when(k == 7)
        def _():
            half = zbuf.shape[2] // 2
            for part in range(2):
                cols = pl.ds(part * half, half)
                remote(
                    zbuf.at[7, :, cols], zbuf.at[7, :, cols], zss.at[0], zrs.at[8 - part], ep, x
                ).wait_recv()

    def select_block(k):
        z_wait(k)

        @pl.when((k >= 1) & (k <= 4))
        def _():
            z_copy(k).start()

        @pl.when(k == 5)
        def _():
            z_copy(5, 1).start()

        @pl.when(k == 6)
        def _():
            z_copy(6, 0).start()

        code = infoz[k, 0]
        want = lax.broadcasted_iota(jnp.int32, (NE, CAP, 128), 1).astype(F32)
        place = (jnp.broadcast_to(code[:, None, :], (NE, CAP, 128)) == want).astype(F32)
        place = place.reshape(NE * CAP, 128).astype(BF16)
        pbuf[k] = place
        block = zbuf[k]
        for q in range(4):
            cols = slice(512 * q, 512 * (q + 1))
            rows = dot(place[:, 0:n_tok], block[:, cols])
            ysend[k, :, :, cols] = rows.astype(BF16).reshape(NE, CAP, 512)
        buf[par, k * NE + yc] = ysend[k, yc]
        for d in (1, 7, 2, 6, 3, 5, 4):
            y_copy(k, d).start()

    half_e = NE // 2

    def x_copy(k, side):
        rows = pl.ds(k * NE + side * half_e, half_e)
        return remote(
            buf.at[par, rows],
            buf.at[par, rows],
            xss.at[k, side],
            xrs.at[k, side],
            ep,
            left if side else right,
        )

    def x_wait(k, side):
        rows = pl.ds(k * NE + side * half_e, half_e)
        remote(
            buf.at[1 - par, rows], buf.at[1 - par, rows], xss.at[k, side], xrs.at[k, side], ep, x
        ).wait_recv()

    def pass_on(k):
        for d in range(1, NE):
            y_wait(k, d)
        x_copy(k, 0).start()
        x_copy(k, 1).start()

    def einfo_copy(d):
        j = (yc + d) % NE
        return remote(infoe.at[j], einfo.at[yc], ess.at[d], ers.at[d], at_e(j), x)

    def einfo_wait(d):
        j = (yc + NE - d) % NE
        remote(infoe.at[0], einfo.at[j], ess.at[d], ers.at[d], ep, x).wait_recv()

    def spread_info():
        for e in range(NE):
            for part in range(2):
                infoe[e, part] = jnp.concatenate(
                    [infoz[k, part, e : e + 1, :] for k in range(NK)], axis=0
                )
        einfo[yc] = infoe[yc]
        for d in range(1, NE):
            einfo_copy(d).start()

    def slot_rows(part, k):
        return jnp.concatenate([einfo[j, part, pl.ds(k, 1), :] for j in range(NE)], axis=0)

    def score_copy(m, d):
        t = (x + d) % 4
        rows = pl.ds(m * 16, 16)
        return remote(sx.at[0, rows], sx.at[4 - d, rows], xcs.at[m, d], xcr.at[m, d], ep, t)

    def score_wait(m, d):
        rows = pl.ds(m * 16, 16)
        remote(sx.at[0, rows], sx.at[4 - d, rows], xcs.at[m, d], xcr.at[m, d], ep, x).wait_recv()

    def halves_copy(m, which, slot):
        k = 2 * m + which
        peer = near_b if which else near_a
        q = far if slot else peer
        rows = pl.ds(k * NE, NE)
        return remote(
            dxq.at[q, rows], r1.at[slot, rows], r1s.at[k, slot], r1r.at[k, slot], ep, peer
        )

    def halves_wait(m, which, slot):
        k = 2 * m + which
        rows = pl.ds(k * NE, NE)
        remote(
            r1.at[slot, rows], r1.at[slot, rows], r1s.at[k, slot], r1r.at[k, slot], ep, x
        ).wait_recv()

    def compute(m):
        for k in (2 * m, 2 * m + 1):
            x_wait(k, 0)
            x_wait(k, 1)
        rows = pl.ds(m * 16, 16)
        flat = pl.ds(pl.multiple_of(m * 128, 128), 128)
        xin = buf[0, rows].reshape(128, 2048)
        gin = buf[1, rows].reshape(128, 2048)
        gate_pre = dot(xin, wg[...])
        up_pre = dot(xin, wu[...])
        back = dot_last(gin, wd[...])
        code = jnp.concatenate([slot_rows(0, 2 * m), slot_rows(0, 2 * m + 1)], axis=0)
        gate = jnp.concatenate([slot_rows(1, 2 * m), slot_rows(1, 2 * m + 1)], axis=0)
        want = lax.broadcasted_iota(jnp.int32, (16, CAP, 128), 1).astype(F32)
        mine = jnp.broadcast_to(code[:, None, :], (16, CAP, 128)) == want
        wide = jnp.where(mine, jnp.broadcast_to(gate[:, None, :], (16, CAP, 128)), 0.0)
        weight = jnp.sum(wide.reshape(128, 128), axis=1, keepdims=True)
        glu = jnp.minimum(gate_pre, 7.0)
        lin1 = jnp.clip(up_pre, -7.0, 7.0) + 1.0
        sig = jax.nn.sigmoid(1.702 * glu)
        act = glu * sig
        hidden = lin1 * act
        slope = lin1 * (sig + 1.702 * glu * sig * (1.0 - sig))
        slope = jnp.where(gate_pre < 7.0, slope, 0.0)
        up_slope = jnp.where((up_pre > -7.0) & (up_pre < 7.0), act, 0.0)
        score = jnp.sum(hidden * back, axis=1, keepdims=True)
        d_hidden = weight * back
        d_gate = (d_hidden * slope).astype(BF16)
        d_up = (d_hidden * up_slope).astype(BF16)
        dgu[flat, 0:384] = d_gate
        dgu[flat, 384:768] = d_up
        wtd[flat, :] = (weight * hidden).astype(BF16)
        lane = lax.broadcasted_iota(jnp.int32, (16, CAP, 128), 2)
        sub = lax.broadcasted_iota(jnp.int32, (16, CAP, 128), 1)
        spread = jnp.broadcast_to(score, (128, 128)).reshape(16, CAP, 128)
        sx[0, rows] = jnp.sum(jnp.where(lane == sub, spread, 0.0), axis=1)
        for d in range(1, 4):
            score_copy(m, d).start()
        for q in range(4):
            cols = slice(512 * q, 512 * (q + 1))
            part = dot_last(d_gate, wg[cols, :]) + dot_last(d_up, wu[cols, :])
            dxq[q, rows] = part.astype(BF16).reshape(16, CAP, 512)
        for slot in (1, 0):
            for which in range(2):
                halves_copy(m, which, slot).start()

    def quarter_copy(m, which):
        k = 2 * m + which
        rows = pl.ds(k * NE, NE)
        return remote(
            s2.at[rows], r2.at[rows], r2s.at[k], r2r.at[k], ep, near_a if which else near_b
        )

    def reduce_first(m):
        for which in range(2):
            k = 2 * m + which
            rows = pl.ds(k * NE, NE)
            halves_wait(m, which, 1)
            s2[rows] = (
                dxq[near_a if which else near_b, rows].astype(F32) + r1[1, rows].astype(F32)
            ).astype(BF16)
            quarter_copy(m, which).start()
        for which in range(2):
            k = 2 * m + which
            rows = pl.ds(k * NE, NE)
            halves_wait(m, which, 0)
            acc[rows] = dxq[x, rows].astype(F32) + r1[0, rows].astype(F32)

    def back_copy(m, d):
        j = (yc + d) % NE
        ks = pl.ds(2 * m, 2)
        return remote(yret.at[j, ks], yrr.at[yc, ks], vss.at[m, d], vrs.at[m, d], at_e(j), x)

    def back_wait(m, d):
        j = (yc + NE - d) % NE
        ks = pl.ds(2 * m, 2)
        remote(yret.at[0, ks], yrr.at[j, ks], vss.at[m, d], vrs.at[m, d], ep, x).wait_recv()

    def reduce_second(m):
        for which in range(2):
            k = 2 * m + which
            rows = pl.ds(k * NE, NE)
            remote(s2.at[rows], r2.at[rows], r2s.at[k], r2r.at[k], ep, x).wait_recv()
            total = (acc[rows] + r2[rows].astype(F32)).astype(BF16)
            for j in range(NE):
                yret[j, k] = total[j]
        yrr[yc, pl.ds(2 * m, 2)] = yret[yc, pl.ds(2 * m, 2)]
        for d in (1, 7, 2, 6, 3, 5, 4):
            back_copy(m, d).start()

    def home_copy(k):
        return remote(
            wsend.at[k], wrecv.at[PAIR_OF[k]], wss.at[k], wrs.at[PAIR_OF[k]], at_z(z_of(k)), x
        )

    def combine(m):
        for d in range(1, NE):
            back_wait(m, d)
        for which in range(2):
            k = 2 * m + which
            rows = jnp.concatenate([yrr[j, k] for j in range(NE)], axis=0)
            wsend[k] = dot_first(pbuf[k][:, 0:n_tok], rows).astype(BF16)
            if k > 0:
                home_copy(k).start()

    for k in range(1, NK):
        info_wait(k)
    spread_info()

    def round_of(it, carry):
        @pl.when(it < NK)
        def _():
            select_block(it)

        @pl.when((it >= 1) & (it <= NK))
        def _():
            pass_on(it - 1)

        @pl.when(it == 3)
        def _():
            load_g.wait()
            load_u.wait()
            load_d.wait()
            for d in range(1, NE):
                einfo_wait(d)

        @pl.when((it >= 3) & (it % 2 == 1))
        def _():
            compute((it - 3) // 2)

        return carry

    lax.fori_loop(0, 10, round_of, 0)

    for m in range(4):
        for d in range(1, 4):
            score_wait(m, d)
    sx[1] = (sx[0] + sx[1]) + (sx[2] + sx[3])

    def sy_copy(d):
        j = (yc + d) % NE
        return remote(sy.at[j], syr.at[yc], sys_.at[d], syr_.at[d], at_e(j), x)

    for j in range(NE):
        sy[j] = jnp.concatenate([sx[1, k * NE + j : k * NE + j + 1, :] for k in range(NK)], axis=0)
    syr[yc] = sy[yc]
    for d in range(1, NE):
        sy_copy(d).start()

    reduce_first(0)
    reduce_first(1)

    def out_copy(i, slot):
        rows = pl.ds(pl.multiple_of(i * 256, 256), 256)
        return (
            pltpu.make_async_copy(
                stage.at[slot, :, pl.ds(0, 384)], gg_hbm.at[rows], outs.at[0, slot]
            ),
            pltpu.make_async_copy(
                stage.at[slot, :, pl.ds(384, 384)], ug_hbm.at[rows], outs.at[1, slot]
            ),
            pltpu.make_async_copy(stage2.at[slot], dg_hbm.at[:, rows], outs.at[2, slot]),
        )

    def weight_tile(i, carry):
        cols = pl.ds(pl.multiple_of(i * 256, 256), 256)
        xs = buf[0, :, :, cols].reshape(512, 256)
        stage[i] = dot_first(xs, dgu[...]).astype(BF16)
        gs = buf[1, :, :, cols].reshape(512, 256)
        stage2[i] = dot_first(wtd[...], gs).astype(BF16)
        for c in out_copy(i, i):
            c.start()
        return carry

    lax.fori_loop(0, 2, weight_tile, 0)

    def sz_copy(k):
        zz = z_of(k)
        return remote(
            szs.at[k],
            smat.at[pl.ds(pl.multiple_of(z * NE, NE), NE)],
            szs_.at[k],
            szr_.at[PAIR_OF[k]],
            at_z(zz),
            x,
        )

    for d in range(1, NE):
        j = (yc + NE - d) % NE
        remote(sy.at[0], syr.at[j], sys_.at[d], syr_.at[d], ep, x).wait_recv()
    for k in range(NK):
        szs[k] = jnp.concatenate([syr[e, k : k + 1, :] for e in range(NE)], axis=0)
    for k in range(1, NK):
        sz_copy(k).start()
    smat[own, :] = szs[0]

    reduce_first(2)
    reduce_first(3)
    reduce_second(0)
    reduce_second(1)
    reduce_second(2)
    reduce_second(3)

    lax.fori_loop(2, 5, weight_tile, 0)

    for k in range(1, NK):
        zz = z_of(k)
        rows = pl.ds(pl.multiple_of(zz * NE, NE), NE)
        remote(szs.at[k], smat.at[rows], szs_.at[k], szr_.at[k], ep, x).wait_recv()
    score_at = jnp.zeros((n_exp, 128), F32)
    for r in range(CAP):
        score_at = score_at + jnp.where(info[0] == float(r), smat[:, r : r + 1], 0.0)
    gate_t = info[1]
    mean = jnp.sum(gate_t * score_at, axis=0, keepdims=True)
    dmat[...] = jnp.where(info[0] >= 0.0, gate_t * (score_at - mean), 0.0)

    def dz_copy(k):
        zz = z_of(k)
        return remote(
            dmat.at[pl.ds(pl.multiple_of(zz * NE, NE), NE)],
            dz.at[PAIR_OF[k]],
            dzs_.at[k],
            dzr_.at[PAIR_OF[k]],
            at_z(zz),
            x,
        )

    for k in range(1, NK):
        dz_copy(k).start()
    dz[0] = dmat[own, :]

    for m in range(4):
        combine(m)

    lax.fori_loop(5, 8, weight_tile, 0)

    def dy_copy(d):
        j = (yc + d) % NE
        return remote(dys.at[j], de.at[yc], dys_.at[d], dyr_.at[d], at_e(j), x)

    for k in range(1, NK):
        remote(dz.at[k], dz.at[k], dzs_.at[k], dzr_.at[k], ep, x).wait_recv()
    for e in range(NE):
        dys[e] = jnp.concatenate([dz[k, e : e + 1, :] for k in range(NK)], axis=0)
    for d in range(1, NE):
        dy_copy(d).start()
    de[yc] = dys[yc]

    d_t = dmat[...]
    d_hi = d_t.astype(BF16)
    d_lo = (d_t - d_hi.astype(F32)).astype(BF16)
    x_rows = pl.ds(pl.multiple_of(x * 512, 512), 512)
    rw_x = rw_ref[x_rows, :]

    def across(d):
        return lax.dot_general(d, rw_x, (((0,), (1,)), ((), ())), preferred_element_type=F32)

    total = (across(d_hi) + across(d_lo))[0:n_tok, :] + wsend[0].astype(F32)
    for k in range(1, NK):
        remote(wsend.at[k], wrecv.at[k], wss.at[k], wrs.at[k], ep, x).wait_recv()
        total = total + wrecv[k].astype(F32)
    tg_ref[...] = total.astype(BF16)

    for d in range(1, NE):
        j = (yc + NE - d) % NE
        remote(dys.at[0], de.at[j], dys_.at[d], dyr_.at[d], ep, x).wait_recv()
    want = lax.broadcasted_iota(jnp.int32, (NE, CAP, 128), 1).astype(F32)
    sums = jnp.zeros((CAP, 512), F32)
    for k in range(NK):
        code = slot_rows(0, k)
        d_rows = jnp.concatenate([de[j, k : k + 1, :] for j in range(NE)], axis=0)
        mine = jnp.broadcast_to(code[:, None, :], (NE, CAP, 128)) == want
        wide = jnp.where(mine, jnp.broadcast_to(d_rows[:, None, :], (NE, CAP, 128)), 0.0)
        slot_d = jnp.sum(wide, axis=2, keepdims=True)
        rows = buf[0, k * NE : (k + 1) * NE, :, x_rows].astype(F32)
        sums = sums + jnp.sum(slot_d * rows, axis=0)
    rg_ref[...] = jnp.sum(sums, axis=0, keepdims=True)

    z_left.wait_send()
    z_right.wait_send()
    for k in (1, 2, 3, 4):
        z_copy(k).wait_send()
    z_copy(5, 1).wait_send()
    z_copy(6, 0).wait_send()
    for k in range(1, NK):
        info_copy(k).wait_send()
        home_copy(k).wait_send()
        sz_copy(k).wait_send()
        dz_copy(k).wait_send()
    for d in range(1, NE):
        einfo_copy(d).wait_send()
        sy_copy(d).wait_send()
        dy_copy(d).wait_send()

    def drain(k, carry):
        for d in range(1, NE):
            y_copy(k, d).wait_send()
        x_copy(k, 0).wait_send()
        x_copy(k, 1).wait_send()
        for c in out_copy(k, k):
            c.wait()
        return carry

    lax.fori_loop(0, NK, drain, 0)
    for m in range(4):
        for d in range(1, 4):
            score_copy(m, d).wait_send()
        for d in range(1, NE):
            back_copy(m, d).wait_send()
        for which in range(2):
            halves_copy(m, which, 0).wait_send()
            halves_copy(m, which, 1).wait_send()
            quarter_copy(m, which).wait_send()


def per_device(tokens, out_grad, expert_ids, router_weight, w_gate, w_up, w_down):
    n_tok, width = tokens.shape
    n_exp = router_weight.shape[1]
    ff = w_gate.shape[2]
    quarter = width // 4
    any_space = pl.BlockSpec(memory_space=pl.ANY)
    vmem = pl.BlockSpec(memory_space=pltpu.VMEM)
    dma = pltpu.SemaphoreType.DMA
    slots = NK * NE
    scratch = [
        pltpu.VMEM((n_tok, width), BF16),
        pltpu.VMEM((width, ff), BF16),
        pltpu.VMEM((width, ff), BF16),
        pltpu.VMEM((ff, width), BF16),
        pltpu.VMEM((NK, n_tok, width), BF16),
        pltpu.VMEM((128, 128), F32),
        pltpu.VMEM((2, n_exp, 128), F32),
        pltpu.VMEM((NK, 2, NE, 128), F32),
        pltpu.VMEM((NE, 2, NK, 128), F32),
        pltpu.VMEM((NE, 2, NK, 128), F32),
        pltpu.VMEM((NK, NE * CAP, 128), BF16),
        pltpu.VMEM((NK, NE, CAP, width), BF16),
        pltpu.VMEM((2, slots, CAP, width), BF16),
        pltpu.VMEM((slots * CAP, 2 * ff), BF16),
        pltpu.VMEM((slots * CAP, ff), BF16),
        pltpu.VMEM((4, slots, CAP, quarter), BF16),
        pltpu.VMEM((2, slots, CAP, quarter), BF16),
        pltpu.VMEM((slots, CAP, quarter), F32),
        pltpu.VMEM((slots, CAP, quarter), BF16),
        pltpu.VMEM((slots, CAP, quarter), BF16),
        pltpu.VMEM((NE, NK, CAP, quarter), BF16),
        pltpu.VMEM((NE, NK, CAP, quarter), BF16),
        pltpu.VMEM((NK, n_tok, quarter), BF16),
        pltpu.VMEM((NK, n_tok, quarter), BF16),
        pltpu.VMEM((4, slots, 128), F32),
        pltpu.VMEM((NE, NK, 128), F32),
        pltpu.VMEM((NE, NK, 128), F32),
        pltpu.VMEM((NK, NE, 128), F32),
        pltpu.VMEM((n_exp, 128), F32),
        pltpu.VMEM((n_exp, 128), F32),
        pltpu.VMEM((NK, NE, 128), F32),
        pltpu.VMEM((NE, NK, 128), F32),
        pltpu.VMEM((NE, NK, 128), F32),
        pltpu.VMEM((8, 256, 2 * ff), BF16),
        pltpu.VMEM((8, ff, 256), BF16),
        dma((8,)),
        dma((8,)),
        dma((9,)),
        dma((8,)),
        dma((8,)),
        dma((8,)),
        dma((8,)),
        dma((8, 8)),
        dma((8, 8)),
        dma((8, 2)),
        dma((8, 2)),
        dma((8, 2)),
        dma((8, 2)),
        dma((8,)),
        dma((8,)),
        dma((4, 4)),
        dma((4, 4)),
        dma((8,)),
        dma((8,)),
        dma((8,)),
        dma((8,)),
        dma((4, 8)),
        dma((4, 8)),
        dma((8,)),
        dma((8,)),
        dma((8,)),
        dma((8,)),
        dma((8,)),
        dma((8,)),
        dma((3, 8)),
    ]
    out = pl.pallas_call(
        step_kernel,
        name="moe_backward",
        out_shape=(
            jax.ShapeDtypeStruct((n_tok, quarter), BF16),
            jax.ShapeDtypeStruct((1, quarter), F32),
            jax.ShapeDtypeStruct((width, ff), BF16),
            jax.ShapeDtypeStruct((width, ff), BF16),
            jax.ShapeDtypeStruct((ff, width), BF16),
        ),
        in_specs=[any_space, any_space, vmem, vmem, any_space, any_space, any_space],
        out_specs=(vmem, vmem, any_space, any_space, any_space),
        scratch_shapes=scratch,
        compiler_params=pltpu.CompilerParams(
            collective_id=0, has_side_effects=True, vmem_limit_bytes=56 * 1024 * 1024
        ),
    )(tokens, out_grad, expert_ids, router_weight, w_gate[0], w_up[0], w_down[0])
    token_grad, router_grad, gate_grad, up_grad, down_grad = out
    return (
        token_grad,
        router_grad.reshape(quarter, 1),
        gate_grad[None],
        up_grad[None],
        down_grad[None],
    )


def solution(mesh):
    in_specs = (
        P("ep", None),
        P("ep", None),
        P("ep", None),
        P(),
        P("ep", None, "tp"),
        P("ep", None, "tp"),
        P("ep", "tp", None),
    )
    out_specs = (
        P("ep", "tp"),
        P("tp", "ep"),
        P("ep", None, "tp"),
        P("ep", None, "tp"),
        P("ep", "tp", None),
    )
    return jax.shard_map(
        per_device, mesh=mesh, in_specs=in_specs, out_specs=out_specs, check_vma=False
    )
```

time: 255 us -> 108 us (0.42)
  Pallas kernels: 0 us -> 93.9 us
  waiting for transfers between devices: 76.3 us -> 0 us
  blocking collectives: 64.8 us -> 0 us
  starting transfers between devices: 26.8 us -> 0 us
  local copies, waits for them, and re-layouts: 38 us -> 11.9 us
  matrix products: 24.2 us -> 0 us
  between operations: 14.6 us -> 0.64 us
  other arithmetic: 9.56 us -> 0 us
    pallas_call x0 -> x1, Pallas kernels: none -> 93.9 us  [per_device(): pl.pallas_call(step_kernel, name='moe_backward', out_shape=(jax.ShapeDtyp...]
    all_to_all x3 -> x0, blocking collectives: 64.8 us -> none  [the longest x1 41.1 us: side_by_side(): lax.all_to_all(both, axis, split_axis=split_dim, concat_axis=concat_dim,...]
    all_to_all x4 -> x0, waiting for transfers between devices: 58.3 us -> none  [the longest x1 26 us: side_by_side_3(): lax.all_to_all(both, axis, split_axis=split_dim, concat_axis=concat_dim,...]
    all_to_all x4 -> x0, starting transfers between devices: 26.7 us -> none  [the longest x1 11.7 us: side_by_side_3(): lax.all_to_all(both, axis, split_axis=split_dim, concat_axis=concat_dim,...]
    dot_general x11 -> x0, matrix products: 24.2 us -> none  [the longest x3 11.9 us: contract_first(): lax.dot_general(left, right, (((0,), (0,)), ((), ())), preferred_element_...]
    all_gather x1 -> x0, waiting for transfers between devices: 17.9 us -> none  [side_by_side_2(): lax.all_gather(both, axis, axis=dim, tiled=True)]
    scatter x3 -> x0, local copies, waits for them, and re-layouts: 14.1 us -> none  [the longest x2 12.9 us: per_device(): jnp.zeros((buffer_rows, model_width), jnp.bfloat16).at[slot_index]]
    unnamed x49 -> x11, local copies, waits for them, and re-layouts: 4.3 us -> 11.9 us
  transfers between devices with their start and end apart: 5 -> 0, of which waited for: 4 -> 0; matrix products, arithmetic and copies ran while one was open for 9% -> 0% of each run, Pallas kernels for 0% -> 0%
where the time goes in v1:
time: 108 us; the launch traced here: 106 us
  Pallas kernels  93.9 us (87%)
  local copies, waits for them, and re-layouts  11.9 us (11%)
    pallas_call x1, Pallas kernels, per_device(): pl.pallas_call(step_kernel, name='moe_backward', out_shape=(jax.ShapeDtyp...  93.9 us
    unnamed x11, local copies, waits for them, and re-layouts  11.9 us

profile of v1, /device:TPU:1, one launch (start us, length us, event | category | flops | bytes accessed | tf_op | source)
XLA Modules:
  0.0 106.5 jit_solution(1818513159685787523)
XLA Ops:
  0.6 1.4 %copy.12.ids_ref = s32[48,4]{1,0:T(8,128)} copy(s32[48,4]{0,1:T(4,128)} %param.9) | data formatting | bytes 1536 | tf_op args[2]
  2.0 2.0 %copy.13.rw_ref = bf16[2048,64]{1,0:T(8,128)(2,1)} copy(bf16[2048,64]{0,1:T(8,128)(2,1)} %param.10) | data formatting | bytes 524288 | tf_op args[3]
  4.0 93.9 %moe_backward.1 = (bf16[48,512]{1,0:T(8,128)(2,1)}, f32[1,512]{1,0:T(1,128)}, bf16[2048,384]{1,0:T(8,128)(2,1)}, bf16[2048,384]{1,0:T(8,128)(2,1)}, bf16[384,2048]{1,0:T(8,128)(2,1)}) custom-call(bf16[48,2048]{1,0:T(8,128)(2,1)} %tok_hbm.1, bf16[48,2048]{1,0:T(8,128)(2,1)} %grad_hbm.1, s32[48,4]{1,0:T(8,128)} %copy.12.ids_ref, ...), custom_call_target="tpu_custom_call" | custom-call | tf_op jit(solution)/shard_map/moe_backward/pallas_call | solution.py:754
  97.9 1.4 %copy.19 = bf16[48,512]{1,0:T(8,128)(2,1)} copy(bf16[48,512]{1,0:T(8,128)(2,1)} %get-tuple-element.20) | data formatting | bytes 98304
  99.3 1.2 %copy.20 = f32[512,1]{0,1:T(1,128)} copy(f32[512,1]{0,1:T(1,128)} %bitcast.13) | data formatting | bytes 4096
  100.5 0.0 copy-start.1
  100.5 2.8 %copy.21 = bf16[1,2048,384]{2,1,0:T(8,128)(2,1)} copy(bf16[1,2048,384]{2,1,0:T(8,128)(2,1)} %bitcast.9) | data formatting | bytes 3145728
  103.4 0.0 copy-done.1
  103.4 0.0 copy-start
  103.4 1.1 %copy.22 = bf16[1,2048,384]{2,1,0:T(8,128)(2,1)} copy(bf16[1,2048,384]{2,1,0:T(8,128)(2,1)S(1)} %bitcast.8) | data formatting | bytes 3145728
  104.5 0.8 copy-done
  105.3 1.1 %copy.23 = bf16[1,384,2048]{2,1,0:T(8,128)(2,1)} copy(bf16[1,384,2048]{2,1,0:T(8,128)(2,1)S(1)} %bitcast.7) | data formatting | bytes 3145728
Async XLA Ops:
  100.5 2.8 %copy-start.1 = (bf16[2048,384]{1,0:T(8,128)(2,1)S(1)}, bf16[2048,384]{1,0:T(8,128)(2,1)}, u32[]{:S(2)}) copy-start(bf16[2048,384]{1,0:T(8,128)(2,1)} %get-tuple-element.13) | copy-start | bytes 4718596
  103.4 2.0 %copy-start = (bf16[384,2048]{1,0:T(8,128)(2,1)S(1)}, bf16[384,2048]{1,0:T(8,128)(2,1)}, u32[]{:S(2)}) copy-start(bf16[384,2048]{1,0:T(8,128)(2,1)} %get-tuple-element.14) | copy-start | bytes 4718596

commit v2 on v1

v2 whole, which is shorter than its diff:
```python
import functools

import jax
import jax.numpy as jnp
from jax import lax
from jax.experimental import pallas as pl
from jax.experimental.pallas import tpu as pltpu
from jax.sharding import PartitionSpec as P

MESH = pl.DeviceIdType.MESH
F32 = jnp.float32
BF16 = jnp.bfloat16
NK = 8
NE = 8
CAP = 8
PAIR_OF = (0, 2, 1, 4, 3, 6, 5, 7)
GROUPS = ((0, 2), (2, 2), (4, 2), (6, 2))


def scoped(f):
    @functools.wraps(f)
    def run(*args):
        with jax.named_scope(f.__name__):
            return f(*args)

    return run


def dot_last(a, b):
    return lax.dot_general(a, b, (((1,), (1,)), ((), ())), preferred_element_type=F32)


def dot_first(a, b):
    return lax.dot_general(a, b, (((0,), (0,)), ((), ())), preferred_element_type=F32)


def dot(a, b):
    return jnp.dot(a, b, preferred_element_type=F32)


def step_kernel(
    tok_hbm,
    grad_hbm,
    ids_hbm,
    rw_hbm,
    wg_hbm,
    wu_hbm,
    wd_hbm,
    tg_ref,
    rg_ref,
    gg_ref,
    ug_ref,
    dg_ref,
    tokv,
    idsv,
    rwv,
    wg,
    wu,
    wd,
    zbuf,
    tiles,
    etiles,
    codes,
    pcodes,
    upper,
    transit,
    pbuf,
    ysend,
    buf,
    dgu,
    wtd,
    dxq,
    r1,
    acc,
    s2,
    r2,
    yret,
    yrr,
    wsend,
    wrecv,
    sx,
    sy,
    syr,
    szs,
    smat,
    dmat,
    means,
    dys,
    de,
    ld,
    sent,
    got,
    zrs,
    irs,
    ers,
    trs,
    yrs,
    xrs,
    r1r,
    r2r,
    vrs,
):
    ep = lax.axis_index("ep")
    x = lax.axis_index("tp")
    z = ep // NE
    yc = ep % NE
    y = yc // 2
    core = yc % 2
    par = x % 2
    odd = x % 2
    near_a = x + 1 - 2 * odd
    near_b = (x + 3 + 2 * odd) % 4
    far = (x + 2) % 4
    right = (x + 1) % 4
    left = (x + 3) % 4

    def remote(src, dst, ss, rs, e, t):
        return pltpu.make_async_remote_copy(
            src_ref=src,
            dst_ref=dst,
            send_sem=ss,
            recv_sem=rs,
            device_id={"ep": e, "tp": t},
            device_id_type=MESH,
        )

    def arrived(ref, sem):
        pltpu.make_async_copy(ref, ref, sem).wait()

    def z_of(k):
        h = (k + 1) // 2
        s = 1 - 2 * ((k + 1) % 2)
        return (z + s * h + NK) % NK

    def at_z(zz):
        return zz * NE + yc

    def at_e(j):
        return z * NE + j

    def in_plane(dy, c):
        return ((y + dy + 4) % 4) * 2 + c

    barrier = pltpu.get_barrier_semaphore()
    for d in (1, NK - 1):
        pl.semaphore_signal(
            barrier, inc=1, device_id={"ep": at_z((z + d) % NK), "tp": x}, device_id_type=MESH
        )
    for d in range(1, NE):
        pl.semaphore_signal(
            barrier, inc=1, device_id={"ep": at_e((yc + d) % NE), "tp": x}, device_id_type=MESH
        )
    for d in range(1, 4):
        pl.semaphore_signal(
            barrier, inc=1, device_id={"ep": ep, "tp": (x + d) % 4}, device_id_type=MESH
        )

    load_tok = pltpu.make_async_copy(tok_hbm, tokv, ld.at[0])
    load_tok.start()
    load_ids = pltpu.make_async_copy(ids_hbm, idsv, ld.at[5])
    load_rw = pltpu.make_async_copy(rw_hbm, rwv, ld.at[6])
    load_ids.start()
    load_rw.start()

    @pl.when(par == 0)
    def _():
        pltpu.make_async_copy(tok_hbm, zbuf.at[0], ld.at[1]).start()

    @pl.when(par == 1)
    def _():
        pltpu.make_async_copy(grad_hbm, zbuf.at[0], ld.at[1]).start()

    load_g = pltpu.make_async_copy(wg_hbm, wg, ld.at[2])
    load_u = pltpu.make_async_copy(wu_hbm, wu, ld.at[3])
    load_d = pltpu.make_async_copy(wd_hbm, wd, ld.at[4])
    load_g.start()
    load_u.start()
    load_d.start()

    @scoped
    def wait_small():
        load_tok.wait()
        load_ids.wait()
        load_rw.wait()

    wait_small()
    n_tok = tokv.shape[0]
    n_exp = rwv.shape[0]
    logits = dot_last(rwv[...], tokv[...])
    expert = lax.broadcasted_iota(jnp.int32, (n_exp, n_tok), 0)
    picked = []
    for k in range(idsv.shape[0]):
        here = idsv[k : k + 1, :] == expert
        picked.append(jnp.sum(jnp.where(here, logits, 0.0), axis=0, keepdims=True))
    picked = jnp.concatenate(picked, axis=0)
    expd = jnp.exp(picked - jnp.max(picked, axis=0, keepdims=True))
    gates = expd / jnp.sum(expd, axis=0, keepdims=True)
    tiles[0] = jnp.full((8, 128), -1.0, F32)
    tiles[0, 0:4, 0:n_tok] = idsv[...].astype(F32)
    tiles[0, 4:8, 0:n_tok] = gates
    row = lax.broadcasted_iota(jnp.int32, (128, 128), 0)
    col = lax.broadcasted_iota(jnp.int32, (128, 128), 1)
    upper[...] = jnp.where(row < col, 1.0, 0.0).astype(BF16)

    def rank_of(hit):
        return jnp.where(hit > 0.0, dot(hit.astype(BF16), upper[...]), -1.0)

    def codes_of(tile, first, count):
        experts = (lax.broadcasted_iota(jnp.int32, (count, 128), 0) + first).astype(F32)
        hit = jnp.zeros((count, 128), F32)
        gate = jnp.zeros((count, 128), F32)
        for k in range(4):
            here = tile[k : k + 1, :] == experts
            hit = hit + jnp.where(here, 1.0, 0.0)
            gate = gate + jnp.where(here, tile[4 + k : 5 + k, :], 0.0)
        return rank_of(hit), gate

    @scoped
    def wait_barrier():
        pl.semaphore_wait(barrier, 2 + (NE - 1) + 3)

    wait_barrier()

    pltpu.make_async_copy(tok_hbm, zbuf.at[0], ld.at[1]).wait()

    half = zbuf.shape[2] // 2

    def z_copy(k, part):
        to = 7 if k >= 5 else k + 2
        s = 1 - 2 * ((k + 1) % 2)
        cols = pl.ds(part * half, half)
        return remote(
            zbuf.at[k, :, cols],
            zbuf.at[to, :, cols],
            sent.at[0],
            zrs.at[to, part],
            at_z((z - s + NK) % NK),
            x,
        )

    def z_first(part, way):
        cols = pl.ds(part * half, half)
        return remote(
            zbuf.at[0, :, cols],
            zbuf.at[1 + way, :, cols],
            sent.at[0],
            zrs.at[1 + way, part],
            at_z((z + 1) % NK) if way else at_z((z + NK - 1) % NK),
            x,
        )

    def tile_copy(k):
        s = 1 - 2 * ((k + 1) % 2)
        return remote(
            tiles.at[k], tiles.at[k + 2], sent.at[1], irs.at[k + 2], at_z((z - s + NK) % NK), x
        )

    below, above = at_z((z + NK - 1) % NK), at_z((z + 1) % NK)
    t_left = remote(tiles.at[0], tiles.at[1], sent.at[1], irs.at[1], below, x)
    t_right = remote(tiles.at[0], tiles.at[2], sent.at[1], irs.at[2], above, x)
    t_left.start()
    t_right.start()
    for part in range(2):
        for way in range(2):
            z_first(part, way).start()

    def share_copy(k, d):
        j = (yc + d) % NE
        return remote(
            tiles.at[k],
            etiles.at[k, pl.ds(pl.multiple_of(yc * 8, 8), 8)],
            sent.at[2],
            ers.at[k],
            at_e(j),
            x,
        )

    def share_wait(k):
        arrived(etiles.at[k, pl.ds(0, 8 * (NE - 1))], ers.at[k])

    steps = ((1, 0), (1, 1), (-1, 0), (-1, 1))

    def transit_copy(k, way):
        e = in_plane(2, way)
        return remote(
            ysend.at[k, e],
            transit.at[k, way],
            sent.at[3],
            trs.at[k],
            at_e(in_plane(-1 if way else 1, core)),
            x,
        )

    def near_copy(k, n):
        j = in_plane(*steps[n]) if n < 4 else in_plane(0, 1 - core)
        return remote(
            ysend.at[k, j], buf.at[par, k * NE + yc], sent.at[4], yrs.at[k], at_e(j), x
        )

    def forward_copy(k, way):
        src = in_plane(1 if way else -1, core)
        return remote(
            transit.at[k, way],
            buf.at[par, k * NE + src],
            sent.at[3],
            yrs.at[k],
            at_e(in_plane(-1 if way else 1, way)),
            x,
        )

    @scoped
    def take(k, part):
        if part == 0:
            arrived(tiles.at[k], irs.at[k])
            if k <= 5:
                tile_copy(k).start()
        cols = pl.ds(part * half, half)
        arrived(zbuf.at[k, :, cols], zrs.at[k, part])
        if k <= 4 or (k, part) in ((5, 1), (6, 0)):
            z_copy(k, part).start()

    @scoped
    def select_block(k):
        for d in range(1, NE):
            share_copy(k, d).start()
        tile = tiles[k]
        etiles[k, pl.ds(pl.multiple_of(yc * 8, 8), 8)] = tile
        code, gate = codes_of(tile, z * NE, NE)
        pcodes[0, k] = code
        pcodes[1, k] = gate
        want = lax.broadcasted_iota(jnp.int32, (NE, CAP, 128), 1).astype(F32)
        place = (jnp.broadcast_to(code[:, None, :], (NE, CAP, 128)) == want).astype(F32)
        place = place.reshape(NE * CAP, 128).astype(BF16)
        pbuf[k] = place
        block = zbuf[k]
        for q in range(4):
            cols = slice(512 * q, 512 * (q + 1))
            rows = dot(place[:, 0:n_tok], block[:, cols])
            ysend[k, :, :, cols] = rows.astype(BF16).reshape(NE, CAP, 512)
        transit_copy(k, 0).start()
        transit_copy(k, 1).start()
        for n in (0, 2, 1, 3, 4):
            near_copy(k, n).start()
        buf[par, k * NE + yc] = ysend[k, yc]

    @scoped
    def hand_over(k):
        arrived(transit.at[k], trs.at[k])
        for way in range(2):
            forward_copy(k, way).start()

    half_e = NE // 2

    def x_copy(k, side):
        rows = pl.ds(k * NE + side * half_e, half_e)
        return remote(
            buf.at[par, rows],
            buf.at[par, rows],
            sent.at[5],
            xrs.at[k],
            ep,
            left if side else right,
        )

    @scoped
    def x_waits(k):
        arrived(buf.at[1 - par, pl.ds(k * NE, NE)], xrs.at[k])

    @scoped
    def y_waits(k):
        arrived(buf.at[par, pl.ds(k * NE, NE - 1)], yrs.at[k])

    @scoped
    def pass_on(k):
        y_waits(k)
        x_copy(k, 0).start()
        x_copy(k, 1).start()

    def slot_info(k):
        hit = jnp.zeros((NE, 128), F32)
        gate = jnp.zeros((NE, 128), F32)
        mine = ep.astype(F32)
        for c in range(4):
            here = etiles[k, pl.ds(c, NE, stride=8), :] == mine
            hit = hit + jnp.where(here, 1.0, 0.0)
            gate = gate + jnp.where(here, etiles[k, pl.ds(4 + c, NE, stride=8), :], 0.0)
        return rank_of(hit), gate

    def score_copy(m, d):
        t = (x + d) % 4
        rows = pl.ds(GROUPS[m][0] * NE, GROUPS[m][1] * NE)
        return remote(sx.at[0, rows], sx.at[4 - d, rows], sent.at[6], got.at[0], ep, t)

    def unit(m, which):
        k, n = GROUPS[m]
        return pl.ds(k * NE + which * n * NE // 2, n * NE // 2)

    def halves_copy(m, which, slot):
        peer = near_b if which else near_a
        q = far if slot else peer
        rows = unit(m, which)
        return remote(
            dxq.at[q, rows], r1.at[slot, rows], sent.at[7], r1r.at[m, slot], ep, peer
        )

    def group(m):
        k, n = GROUPS[m]
        return pl.ds(k * NE, n * NE)

    @scoped
    def compute(m):
        first, count = GROUPS[m]
        n_rows = count * NE * CAP
        infos = []
        for k in range(first, first + count):
            share_wait(k)
            infos.append(slot_info(k))
            codes[0, k], codes[1, k] = infos[-1]
        code = jnp.concatenate([i[0] for i in infos], axis=0)
        gate = jnp.concatenate([i[1] for i in infos], axis=0)
        shape = (count * NE, CAP, 128)
        want = lax.broadcasted_iota(jnp.int32, shape, 1).astype(F32)
        mine = jnp.broadcast_to(code[:, None, :], shape) == want
        wide = jnp.where(mine, jnp.broadcast_to(gate[:, None, :], shape), 0.0)
        weight = jnp.sum(wide.reshape(n_rows, 128), axis=1, keepdims=True)
        for k in range(first, first + count):
            x_waits(k)
        rows = pl.ds(first * NE, count * NE)
        flat = pl.ds(first * NE * CAP, n_rows)
        xin = buf[0, rows].reshape(n_rows, 2048)
        gin = buf[1, rows].reshape(n_rows, 2048)
        gate_pre = dot(xin, wg[...])
        up_pre = dot(xin, wu[...])
        back = dot_last(gin, wd[...])
        glu = jnp.minimum(gate_pre, 7.0)
        lin1 = jnp.clip(up_pre, -7.0, 7.0) + 1.0
        sig = jax.nn.sigmoid(1.702 * glu)
        act = glu * sig
        hidden = lin1 * act
        slope = lin1 * (sig + 1.702 * glu * sig * (1.0 - sig))
        slope = jnp.where(gate_pre < 7.0, slope, 0.0)
        up_slope = jnp.where((up_pre > -7.0) & (up_pre < 7.0), act, 0.0)
        score = jnp.sum(hidden * back, axis=1, keepdims=True)
        d_hidden = weight * back
        d_gate = (d_hidden * slope).astype(BF16)
        d_up = (d_hidden * up_slope).astype(BF16)
        dgu[flat, 0:384] = d_gate
        dgu[flat, 384:768] = d_up
        wtd[flat, :] = (weight * hidden).astype(BF16)
        lane = lax.broadcasted_iota(jnp.int32, shape, 2)
        sub = lax.broadcasted_iota(jnp.int32, shape, 1)
        spread = jnp.broadcast_to(score, (n_rows, 128)).reshape(shape)
        sx[0, rows] = jnp.sum(jnp.where(lane == sub, spread, 0.0), axis=1)
        for d in range(1, 4):
            score_copy(m, d).start()

        for q in range(4):
            cols = slice(512 * q, 512 * (q + 1))
            part = dot_last(d_gate, wg[cols, :]) + dot_last(d_up, wu[cols, :])
            dxq[q, rows] = part.astype(BF16).reshape(count * NE, CAP, 512)
        for slot in (1, 0):
            for which in range(2):
                halves_copy(m, which, slot).start()

    def quarter_copy(m, which):
        rows = unit(m, which)
        return remote(
            s2.at[rows], r2.at[rows], sent.at[8], r2r.at[m], ep, near_a if which else near_b
        )

    @scoped
    def wait_half(m, slot):
        arrived(r1.at[slot, group(m)], r1r.at[m, slot])

    @scoped
    def wait_quarter(m):
        arrived(r2.at[group(m)], r2r.at[m])

    @scoped
    def reduce_first(m):
        wait_half(m, 1)
        for which in range(2):
            rows = unit(m, which)
            s2[rows] = (
                dxq[near_a if which else near_b, rows].astype(F32) + r1[1, rows].astype(F32)
            ).astype(BF16)
            quarter_copy(m, which).start()
        wait_half(m, 0)
        for which in range(2):
            rows = unit(m, which)
            acc[rows] = dxq[x, rows].astype(F32) + r1[0, rows].astype(F32)

    def back_copy(m, d):
        j = (yc + d) % NE
        ks = pl.ds(*GROUPS[m])
        return remote(yret.at[j, ks], yrr.at[yc, ks], sent.at[9], vrs.at[m], at_e(j), x)

    @scoped
    def reduce_second(m):
        first, count = GROUPS[m]
        wait_quarter(m)
        for k in range(first, first + count):
            rows = pl.ds(k * NE, NE)
            total = (acc[rows] + r2[rows].astype(F32)).astype(BF16)
            for j in range(NE):
                yret[j, k] = total[j]
        for d in (1, 7, 2, 6, 3, 5, 4):
            back_copy(m, d).start()
        ks = pl.ds(first, count)
        yrr[yc, ks] = yret[yc, ks]

    def home_copy(k):
        return remote(
            wsend.at[k], wrecv.at[PAIR_OF[k]], sent.at[10], got.at[1], at_z(z_of(k)), x
        )

    @scoped
    def back_waits(m):
        arrived(yrr.at[pl.ds(0, NE - 1), pl.ds(*GROUPS[m])], vrs.at[m])

    @scoped
    def combine(m):
        back_waits(m)
        first, count = GROUPS[m]
        for k in range(first, first + count):
            rows = jnp.concatenate([yrr[j, k] for j in range(NE)], axis=0)
            wsend[k] = dot_first(pbuf[k][:, 0:n_tok], rows).astype(BF16)
            if k > 0:
                home_copy(k).start()

    def both(f, *ks):
        for k in ks:
            f(k)

    def takes(part, *ks):
        for k in ks:
            take(k, part)

    select_block(0)
    takes(0, 1, 2)
    hand_over(0)
    takes(1, 1, 2)
    select_block(1)
    select_block(2)
    pass_on(0)
    takes(0, 3, 4)
    hand_over(1)
    takes(1, 3, 4)
    select_block(3)
    hand_over(2)
    pass_on(1)
    select_block(4)
    takes(0, 5, 6)
    hand_over(3)
    pass_on(2)
    takes(1, 5, 6)
    select_block(5)
    hand_over(4)
    pass_on(3)
    select_block(6)
    take(7, 0)
    take(7, 1)
    load_g.wait()
    load_u.wait()
    load_d.wait()
    compute(0)
    hand_over(5)
    pass_on(4)
    select_block(7)
    hand_over(6)
    pass_on(5)
    compute(1)
    hand_over(7)
    pass_on(6)
    pass_on(7)
    reduce_first(0)
    compute(2)
    reduce_first(1)
    compute(3)
    reduce_second(0)

    @scoped
    def weight_tile(i, carry):
        cols = pl.ds(pl.multiple_of(i * 256, 256), 256)
        xs = buf[0, :, :, cols].reshape(512, 256)
        both = dot_first(xs, dgu[...]).astype(BF16)
        gg_ref[cols, :] = both[:, 0:384]
        ug_ref[cols, :] = both[:, 384:768]
        gs = buf[1, :, :, cols].reshape(512, 256)
        dg_ref[:, cols] = dot_first(wtd[...], gs).astype(BF16)
        return carry

    def weight_tiles(a, b):
        lax.fori_loop(a, b, weight_tile, 0)

    def sy_copy(d):
        j = (yc + d) % NE
        return remote(sy.at[j], syr.at[yc], sent.at[11], got.at[2], at_e(j), x)

    @scoped
    def scores_x():
        arrived(sx.at[pl.ds(1, 3)], got.at[0])
        sx[1] = (sx[0] + sx[1]) + (sx[2] + sx[3])
        for j in range(NE):
            sy[j] = jnp.concatenate(
                [sx[1, k * NE + j : k * NE + j + 1, :] for k in range(NK)], axis=0
            )
        for d in range(1, NE):
            sy_copy(d).start()
        syr[yc] = sy[yc]

    def sz_copy(k):
        return remote(
            szs.at[k],
            smat.at[pl.ds(pl.multiple_of(z * NE, NE), NE)],
            sent.at[12],
            got.at[3],
            at_z(z_of(k)),
            x,
        )

    def mean_copy(k):
        return remote(
            means.at[0],
            means.at[PAIR_OF[k]],
            sent.at[13],
            got.at[4],
            at_z(z_of(k)),
            x,
        )

    def at_ranks(code, scores):
        found = jnp.zeros(code.shape, F32)
        for r in range(CAP):
            found = found + jnp.where(code == float(r), scores[:, r : r + 1], 0.0)
        return found

    @scoped
    def scores_y():
        arrived(syr.at[pl.ds(0, NE - 1)], got.at[2])
        for k in range(NK):
            szs[k] = jnp.concatenate([syr[e, k : k + 1, :] for e in range(NE)], axis=0)
            part = pcodes[1, k] * at_ranks(pcodes[0, k], szs[k])
            means[0, pl.ds(z_of(k), 1), :] = jnp.sum(part, axis=0, keepdims=True)
        for k in range(1, NK):
            mean_copy(k).start()
        for k in range(1, NK):
            sz_copy(k).start()
        smat[pl.ds(pl.multiple_of(z * NE, NE), NE), :] = szs[0]

    def dy_copy(d):
        j = (yc + d) % NE
        return remote(dys, de.at[yc], sent.at[14], got.at[5], at_e(j), x)

    @scoped
    def scores_z():
        arrived(means.at[pl.ds(1, NK - 1)], got.at[4])
        total = means[0]
        for k in range(1, NK):
            total = total + means[k]
        dys[...] = total
        for d in range(1, NE):
            dy_copy(d).start()
        de[yc] = total

    @scoped
    def home_logits():
        arrived(smat.at[pl.ds(0, NE * (NK - 1))], got.at[3])
        code_t, gate_t = codes_of(tiles[0], 0, n_exp)
        score_at = at_ranks(code_t, smat)
        mean = jnp.sum(gate_t * score_at, axis=0, keepdims=True)
        dmat[...] = jnp.where(code_t >= 0.0, gate_t * (score_at - mean), 0.0)

    x_rows = pl.ds(pl.multiple_of(x * 512, 512), 512)

    @scoped
    def token_out():
        d_t = dmat[...]
        d_hi = d_t.astype(BF16)
        d_lo = (d_t - d_hi.astype(F32)).astype(BF16)
        rw_x = rwv[:, x_rows]
        total = (dot_first(d_hi, rw_x) + dot_first(d_lo, rw_x))[0:n_tok, :]
        total = total + wsend[0].astype(F32)
        arrived(wrecv.at[pl.ds(1, NK - 1)], got.at[1])
        for k in range(1, NK):
            total = total + wrecv[k].astype(F32)
        tg_ref[...] = total.astype(BF16)

    @scoped
    def router_out():
        arrived(de.at[pl.ds(0, NE - 1)], got.at[5])
        shape = (NE, CAP, 128)
        want = lax.broadcasted_iota(jnp.int32, shape, 1).astype(F32)
        lane = lax.broadcasted_iota(jnp.int32, shape, 2)
        sub = lax.broadcasted_iota(jnp.int32, shape, 1)
        sums = jnp.zeros((CAP, 512), F32)

        def of_slots(mask, rows):
            wide = jnp.where(mask, jnp.broadcast_to(rows[:, None, :], shape), 0.0)
            return jnp.sum(wide, axis=2, keepdims=True)

        for k in range(NK):
            mean = jnp.concatenate([de[j, pl.ds(z_of(k), 1), :] for j in range(NE)], axis=0)
            code, gate = codes[0, k], codes[1, k]
            mine = jnp.broadcast_to(code[:, None, :], shape) == want
            score = of_slots(lane == sub, sx[1, k * NE : (k + 1) * NE, :])
            slot_d = of_slots(mine, gate) * (score - of_slots(mine, mean))
            rows = buf[0, k * NE : (k + 1) * NE, :, x_rows].astype(F32)
            sums = sums + jnp.sum(slot_d * rows, axis=0)
        rg_ref[...] = jnp.sum(sums, axis=0, keepdims=True)

    reduce_second(1)
    reduce_first(2)
    weight_tiles(0, 1)
    scores_x()
    combine(0)
    weight_tiles(1, 2)
    reduce_first(3)
    combine(1)
    reduce_second(2)
    scores_y()
    weight_tiles(2, 3)
    reduce_second(3)
    combine(2)
    weight_tiles(3, 5)
    combine(3)
    scores_z()
    weight_tiles(5, 8)
    home_logits()
    router_out()
    token_out()

    with jax.named_scope("drain_all"):
        seven = pl.ds(0, 7)
        for i, ref in enumerate(
            (
                zbuf.at[seven],
                tiles.at[seven],
                etiles.at[seven, pl.ds(0, 64)],
                ysend.at[pl.ds(0, 4)],
                ysend.at[pl.ds(0, 5)],
                buf.at[0],
                sx.at[pl.ds(0, 3)],
                r1,
                s2,
                yret.at[seven],
                wsend.at[seven],
                sy.at[seven],
                szs.at[seven],
                means.at[seven],
                means.at[seven],
            )
        ):
            arrived(ref, sent.at[i])


def finish_kernel(tg, rg, gg, ug, dg, tg_o, rg_o, gg_o, ug_o, dg_o, sems):
    pairs = ((gg, gg_o), (ug, ug_o), (dg, dg_o), (tg, tg_o), (rg, rg_o))
    copies = [pltpu.make_async_copy(a, b, sems.at[i]) for i, (a, b) in enumerate(pairs)]
    for c in copies:
        c.start()
    for c in copies:
        c.wait()


def per_device(tokens, out_grad, expert_ids, router_weight, w_gate, w_up, w_down):
    n_tok, width = tokens.shape
    n_exp = router_weight.shape[1]
    top_count = expert_ids.shape[1]
    ff = w_gate.shape[2]
    quarter = width // 4
    any_space = pl.BlockSpec(memory_space=pl.ANY)
    vmem = pl.BlockSpec(memory_space=pltpu.VMEM)
    hbm = pl.BlockSpec(memory_space=pltpu.HBM)
    dma = pltpu.SemaphoreType.DMA
    slots = NK * NE
    scratch = [
        pltpu.VMEM((n_tok, width), BF16),
        pltpu.VMEM((top_count, n_tok), jnp.int32),
        pltpu.VMEM((n_exp, width), BF16),
        pltpu.VMEM((width, ff), BF16),
        pltpu.VMEM((width, ff), BF16),
        pltpu.VMEM((ff, width), BF16),
        pltpu.VMEM((NK, n_tok, width), BF16),
        pltpu.VMEM((NK, 8, 128), F32),
        pltpu.VMEM((NK, NE * 8, 128), F32),
        pltpu.VMEM((2, NK, NE, 128), F32),
        pltpu.VMEM((2, NK, NE, 128), F32),
        pltpu.VMEM((128, 128), BF16),
        pltpu.VMEM((NK, 2, CAP, width), BF16),
        pltpu.VMEM((NK, NE * CAP, 128), BF16),
        pltpu.VMEM((NK, NE, CAP, width), BF16),
        pltpu.VMEM((2, slots, CAP, width), BF16),
        pltpu.VMEM((slots * CAP, 2 * ff), BF16),
        pltpu.VMEM((slots * CAP, ff), BF16),
        pltpu.VMEM((4, slots, CAP, quarter), BF16),
        pltpu.VMEM((2, slots, CAP, quarter), BF16),
        pltpu.VMEM((slots, CAP, quarter), F32),
        pltpu.VMEM((slots, CAP, quarter), BF16),
        pltpu.VMEM((slots, CAP, quarter), BF16),
        pltpu.VMEM((NE, NK, CAP, quarter), BF16),
        pltpu.VMEM((NE, NK, CAP, quarter), BF16),
        pltpu.VMEM((NK, n_tok, quarter), BF16),
        pltpu.VMEM((NK, n_tok, quarter), BF16),
        pltpu.VMEM((4, slots, 128), F32),
        pltpu.VMEM((NE, NK, 128), F32),
        pltpu.VMEM((NE, NK, 128), F32),
        pltpu.VMEM((NK, NE, 128), F32),
        pltpu.VMEM((n_exp, 128), F32),
        pltpu.VMEM((n_exp, 128), F32),
        pltpu.VMEM((NK, NK, 128), F32),
        pltpu.VMEM((NK, 128), F32),
        pltpu.VMEM((NE, NK, 128), F32),
        dma((7,)),
        dma((15,)),
        dma((6,)),
        dma((8, 2)),
        dma((8,)),
        dma((8,)),
        dma((8,)),
        dma((8,)),
        dma((8,)),
        dma((4, 2)),
        dma((4,)),
        dma((4,)),
    ]
    shapes = (
        jax.ShapeDtypeStruct((n_tok, quarter), BF16),
        jax.ShapeDtypeStruct((1, quarter), F32),
        jax.ShapeDtypeStruct((width, ff), BF16),
        jax.ShapeDtypeStruct((width, ff), BF16),
        jax.ShapeDtypeStruct((ff, width), BF16),
    )
    out = pl.pallas_call(
        step_kernel,
        name="moe_backward",
        out_shape=shapes,
        in_specs=[hbm] * 7,
        out_specs=(vmem,) * 5,
        scratch_shapes=scratch,
        compiler_params=pltpu.CompilerParams(
            collective_id=0, has_side_effects=True, vmem_limit_bytes=40 * 1024 * 1024
        ),
    )(
        *(
            pltpu.with_memory_space_constraint(a, pltpu.HBM)
            for a in (
                tokens,
                out_grad,
                expert_ids.T,
                router_weight.T,
                w_gate[0],
                w_up[0],
                w_down[0],
            )
        )
    )
    token_grad, router_grad, gate_grad, up_grad, down_grad = pl.pallas_call(
        finish_kernel,
        name="finish",
        out_shape=shapes,
        in_specs=[any_space] * 5,
        out_specs=(any_space,) * 5,
        scratch_shapes=[dma((5,))],
        compiler_params=pltpu.CompilerParams(vmem_limit_bytes=4 * 1024 * 1024),
    )(*out)
    return (
        token_grad,
        router_grad.reshape(quarter, 1),
        gate_grad[None],
        up_grad[None],
        down_grad[None],
    )


def solution(mesh):
    in_specs = (
        P("ep", None),
        P("ep", None),
        P("ep", None),
        P(),
        P("ep", None, "tp"),
        P("ep", None, "tp"),
        P("ep", "tp", None),
    )
    out_specs = (
        P("ep", "tp"),
        P("tp", "ep"),
        P("ep", None, "tp"),
        P("ep", None, "tp"),
        P("ep", "tp", None),
    )
    return jax.shard_map(
        per_device, mesh=mesh, in_specs=in_specs, out_specs=out_specs, check_vma=False
    )
```

time: 108 us -> 82.6 us (0.76)
  Pallas kernels: 93.9 us -> 81.1 us
  local copies, waits for them, and re-layouts: 11.9 us -> 0 us
    pallas_call x1 -> x2, Pallas kernels: 93.9 us -> 81.1 us  [the longest x1 78.9 us: per_device(): pl.pallas_call(step_kernel, name='moe_backward', out_shape=shapes, in_spe...]
    unnamed x11 -> x0, local copies, waits for them, and re-layouts: 11.9 us -> none
where the time goes in v2:
time: 82.6 us; the launch traced here: 81.8 us
  Pallas kernels  81.1 us (98%)
    pallas_call x1, Pallas kernels, per_device(): pl.pallas_call(step_kernel, name='moe_backward', out_shape=shapes, in_spe...  78.9 us
    pallas_call x1, Pallas kernels, per_device(): pl.pallas_call(finish_kernel, name='finish', out_shape=shapes, in_specs=[...  2.23 us

profile of v2, /device:TPU:1, one launch (start us, length us, event | category | flops | bytes accessed | tf_op | source)
XLA Modules:
  0.0 81.8 jit_solution(8646502380993088407)
XLA Ops:
  0.6 78.9 %moe_backward.1 = (bf16[48,512]{1,0:T(8,128)(2,1)S(1)}, f32[1,512]{1,0:T(1,128)S(1)}, bf16[2048,384]{1,0:T(8,128)(2,1)S(1)}, bf16[2048,384]{1,0:T(8,128)(2,1)S(1)}, bf16[384,2048]{1,0:T(8,128)(2,1)S(1)}) custom-call(bf16[48,2048]{1,0:T(8,128)(2,1)} %tok_hbm.1, bf16[48,2048]{1,0:T(8,128)(2,1)} %grad_hbm.1, s32[4,48]{1,0:T(4,128)} %bitcast.13, ...), custom_call_target="tpu_custom_call" | custom-call | tf_op jit(solution)/shard_map/moe_backward/pallas_call | solution.py:834
  79.5 2.2 %finish.1 = (bf16[48,512]{1,0:T(8,128)(2,1)}, f32[1,512]{1,0:T(1,128)}, bf16[2048,384]{1,0:T(8,128)(2,1)}, bf16[2048,384]{1,0:T(8,128)(2,1)}, bf16[384,2048]{1,0:T(8,128)(2,1)}) custom-call(bf16[48,512]{1,0:T(8,128)(2,1)S(1)} %get-tuple-element.15.tg, f32[1,512]{1,0:T(1,128)S(1)} %get-tuple-element.16.rg, bf16[2048,384]{1,0:T(8,128)(2,1)S(1)} %get-tuple-element.17.gg, ...), custom_call_target="tpu_custom_call" | custom-call | tf_op jit(solution)/shard_map/finish/pallas_call | solution.py:858

commit v3 on v2

--- a/solution.py
+++ b/solution.py
@@ -15,6 +15,15 @@
 CAP = 8
 PAIR_OF = (0, 2, 1, 4, 3, 6, 5, 7)
 GROUPS = ((0, 2), (2, 2), (4, 2), (6, 2))
+DIRECT = (1, 2)
+
+
+def place_of(k):
+    return (k + NK - 1) % NK
+
+
+def block_at(n):
+    return (n + 1) % NK
 
 
 def scoped(f):
@@ -183,6 +192,51 @@
         load_ids.wait()
         load_rw.wait()
 
+    @scoped
+    def wait_barrier():
+        pl.semaphore_wait(barrier, 2 + (NE - 1) + 3)
+
+    wait_barrier()
+
+    pltpu.make_async_copy(tok_hbm, zbuf.at[0], ld.at[1]).wait()
+
+    half = zbuf.shape[2] // 2
+
+    def z_copy(k, part):
+        to = 7 if k >= 5 else k + 2
+        s = 1 - 2 * ((k + 1) % 2)
+        cols = pl.ds(part * half, half)
+        return remote(
+            zbuf.at[k, :, cols],
+            zbuf.at[to, :, cols],
+            sent.at[0],
+            zrs.at[to, part],
+            at_z((z - s + NK) % NK),
+            x,
+        )
+
+    def z_first(part, way):
+        cols = pl.ds(part * half, half)
+        return remote(
+            zbuf.at[0, :, cols],
+            zbuf.at[1 + way, :, cols],
+            sent.at[0],
+            zrs.at[1 + way, part],
+            at_z((z + 1) % NK) if way else at_z((z + NK - 1) % NK),
+            x,
+        )
+
+    def tile_copy(k):
+        s = 1 - 2 * ((k + 1) % 2)
+        return remote(
+            tiles.at[k], tiles.at[k + 2], sent.at[1], irs.at[k + 2], at_z((z - s + NK) % NK), x
+        )
+
+    below, above = at_z((z + NK - 1) % NK), at_z((z + 1) % NK)
+    t_left = remote(tiles.at[0], tiles.at[1], sent.at[1], irs.at[1], below, x)
+    t_right = remote(tiles.at[0], tiles.at[2], sent.at[1], irs.at[2], above, x)
+    z_first(0, 0).start()
+    z_first(0, 1).start()
     wait_small()
     n_tok = tokv.shape[0]
     n_exp = rwv.shape[0]
@@ -215,54 +269,10 @@
             gate = gate + jnp.where(here, tile[4 + k : 5 + k, :], 0.0)
         return rank_of(hit), gate
 
-    @scoped
-    def wait_barrier():
-        pl.semaphore_wait(barrier, 2 + (NE - 1) + 3)
-
-    wait_barrier()
-
-    pltpu.make_async_copy(tok_hbm, zbuf.at[0], ld.at[1]).wait()
-
-    half = zbuf.shape[2] // 2
-
-    def z_copy(k, part):
-        to = 7 if k >= 5 else k + 2
-        s = 1 - 2 * ((k + 1) % 2)
-        cols = pl.ds(part * half, half)
-        return remote(
-            zbuf.at[k, :, cols],
-            zbuf.at[to, :, cols],
-            sent.at[0],
-            zrs.at[to, part],
-            at_z((z - s + NK) % NK),
-            x,
-        )
-
-    def z_first(part, way):
-        cols = pl.ds(part * half, half)
-        return remote(
-            zbuf.at[0, :, cols],
-            zbuf.at[1 + way, :, cols],
-            sent.at[0],
-            zrs.at[1 + way, part],
-            at_z((z + 1) % NK) if way else at_z((z + NK - 1) % NK),
-            x,
-        )
-
-    def tile_copy(k):
-        s = 1 - 2 * ((k + 1) % 2)
-        return remote(
-            tiles.at[k], tiles.at[k + 2], sent.at[1], irs.at[k + 2], at_z((z - s + NK) % NK), x
-        )
-
-    below, above = at_z((z + NK - 1) % NK), at_z((z + 1) % NK)
-    t_left = remote(tiles.at[0], tiles.at[1], sent.at[1], irs.at[1], below, x)
-    t_right = remote(tiles.at[0], tiles.at[2], sent.at[1], irs.at[2], above, x)
     t_left.start()
     t_right.start()
-    for part in range(2):
-        for way in range(2):
-            z_first(part, way).start()
+    z_first(1, 0).start()
+    z_first(1, 1).start()
 
     def share_copy(k, d):
         j = (yc + d) % NE
@@ -280,7 +290,7 @@
 
     steps = ((1, 0), (1, 1), (-1, 0), (-1, 1))
 
-    def transit_copy(k, way):
+    def transit_copy(k, way, cols):
         e = in_plane(2, way)
         return remote(
             ysend.at[k, e],
@@ -291,17 +301,33 @@
             x,
         )
 
-    def near_copy(k, n):
+    def direct_copy(k, way, cols):
+        e = in_plane(2, way)
+        return remote(
+            ysend.at[k, e, :, cols],
+            buf.at[par, place_of(k) * NE + yc, :, cols],
+            sent.at[4],
+            yrs.at[k],
+            at_e(e),
+            x,
+        )
+
+    def near_copy(k, n, cols):
         j = in_plane(*steps[n]) if n < 4 else in_plane(0, 1 - core)
         return remote(
-            ysend.at[k, j], buf.at[par, k * NE + yc], sent.at[4], yrs.at[k], at_e(j), x
+            ysend.at[k, j, :, cols],
+            buf.at[par, place_of(k) * NE + yc, :, cols],
+            sent.at[4],
+            yrs.at[k],
+            at_e(j),
+            x,
         )
 
     def forward_copy(k, way):
         src = in_plane(1 if way else -1, core)
         return remote(
             transit.at[k, way],
-            buf.at[par, k * NE + src],
+            buf.at[par, place_of(k) * NE + src],
             sent.at[3],
             yrs.at[k],
             at_e(in_plane(-1 if way else 1, way)),
@@ -321,6 +347,10 @@
 
     @scoped
     def select_block(k):
+        place_block(k)
+        send_rows(k, slice(0, 2 * half))
+
+    def place_block(k):
         for d in range(1, NE):
             share_copy(k, d).start()
         tile = tiles[k]
@@ -330,18 +360,18 @@
         pcodes[1, k] = gate
         want = lax.broadcasted_iota(jnp.int32, (NE, CAP, 128), 1).astype(F32)
         place = (jnp.broadcast_to(code[:, None, :], (NE, CAP, 128)) == want).astype(F32)
-        place = place.reshape(NE * CAP, 128).astype(BF16)
-        pbuf[k] = place
-        block = zbuf[k]
-        for q in range(4):
-            cols = slice(512 * q, 512 * (q + 1))
-            rows = dot(place[:, 0:n_tok], block[:, cols])
-            ysend[k, :, :, cols] = rows.astype(BF16).reshape(NE, CAP, 512)
-        transit_copy(k, 0).start()
-        transit_copy(k, 1).start()
+        pbuf[k] = place.reshape(NE * CAP, 128).astype(BF16)
+
+    def send_rows(k, cols):
+        place = pbuf[k]
+        for q in range(cols.start, cols.stop, 512):
+            rows = dot(place[:, 0:n_tok], zbuf[k, :, q : q + 512])
+            ysend[k, :, :, q : q + 512] = rows.astype(BF16).reshape(NE, CAP, 512)
+        for way in range(2):
+            (direct_copy if k in DIRECT else transit_copy)(k, way, cols).start()
         for n in (0, 2, 1, 3, 4):
-            near_copy(k, n).start()
-        buf[par, k * NE + yc] = ysend[k, yc]
+            near_copy(k, n, cols).start()
+        buf[par, place_of(k) * NE + yc, :, cols] = ysend[k, yc, :, cols]
 
     @scoped
     def hand_over(k):
@@ -352,7 +382,7 @@
     half_e = NE // 2
 
     def x_copy(k, side):
-        rows = pl.ds(k * NE + side * half_e, half_e)
+        rows = pl.ds(place_of(k) * NE + side * half_e, half_e)
         return remote(
             buf.at[par, rows],
             buf.at[par, rows],
@@ -364,11 +394,11 @@
 
     @scoped
     def x_waits(k):
-        arrived(buf.at[1 - par, pl.ds(k * NE, NE)], xrs.at[k])
+        arrived(buf.at[1 - par, pl.ds(place_of(k) * NE, NE)], xrs.at[k])
 
     @scoped
     def y_waits(k):
-        arrived(buf.at[par, pl.ds(k * NE, NE - 1)], yrs.at[k])
+        arrived(buf.at[par, pl.ds(place_of(k) * NE, NE - 1)], yrs.at[k])
 
     @scoped
     def pass_on(k):
@@ -412,10 +442,10 @@
         first, count = GROUPS[m]
         n_rows = count * NE * CAP
         infos = []
-        for k in range(first, first + count):
-            share_wait(k)
-            infos.append(slot_info(k))
-            codes[0, k], codes[1, k] = infos[-1]
+        for n in range(first, first + count):
+            share_wait(block_at(n))
+            infos.append(slot_info(block_at(n)))
+            codes[0, n], codes[1, n] = infos[-1]
         code = jnp.concatenate([i[0] for i in infos], axis=0)
         gate = jnp.concatenate([i[1] for i in infos], axis=0)
         shape = (count * NE, CAP, 128)
@@ -423,8 +453,8 @@
         mine = jnp.broadcast_to(code[:, None, :], shape) == want
         wide = jnp.where(mine, jnp.broadcast_to(gate[:, None, :], shape), 0.0)
         weight = jnp.sum(wide.reshape(n_rows, 128), axis=1, keepdims=True)
-        for k in range(first, first + count):
-            x_waits(k)
+        for n in range(first, first + count):
+            x_waits(block_at(n))
         rows = pl.ds(first * NE, count * NE)
         flat = pl.ds(first * NE * CAP, n_rows)
         xin = buf[0, rows].reshape(n_rows, 2048)
@@ -458,6 +488,8 @@
             cols = slice(512 * q, 512 * (q + 1))
             part = dot_last(d_gate, wg[cols, :]) + dot_last(d_up, wu[cols, :])
             dxq[q, rows] = part.astype(BF16).reshape(count * NE, CAP, 512)
+    @scoped
+    def send_halves(m):
         for slot in (1, 0):
             for which in range(2):
                 halves_copy(m, which, slot).start()
@@ -522,8 +554,9 @@
     def combine(m):
         back_waits(m)
         first, count = GROUPS[m]
-        for k in range(first, first + count):
-            rows = jnp.concatenate([yrr[j, k] for j in range(NE)], axis=0)
+        for n in range(first, first + count):
+            k = block_at(n)
+            rows = jnp.concatenate([yrr[j, n] for j in range(NE)], axis=0)
             wsend[k] = dot_first(pbuf[k][:, 0:n_tok], rows).astype(BF16)
             if k > 0:
                 home_copy(k).start()
@@ -536,48 +569,52 @@
         for k in ks:
             take(k, part)
 
+    first_half, second_half = slice(0, half), slice(half, 2 * half)
     select_block(0)
+    hand_over(0)
     takes(0, 1, 2)
-    hand_over(0)
+    place_block(1)
+    send_rows(1, first_half)
+    place_block(2)
+    send_rows(2, first_half)
     takes(1, 1, 2)
-    select_block(1)
-    select_block(2)
+    send_rows(1, second_half)
+    send_rows(2, second_half)
+    takes(0, 3, 4)
     pass_on(0)
-    takes(0, 3, 4)
-    hand_over(1)
     takes(1, 3, 4)
     select_block(3)
-    hand_over(2)
     pass_on(1)
     select_block(4)
+    pass_on(2)
+    hand_over(3)
     takes(0, 5, 6)
-    hand_over(3)
-    pass_on(2)
+    hand_over(4)
     takes(1, 5, 6)
     select_block(5)
-    hand_over(4)
     pass_on(3)
     select_block(6)
     take(7, 0)
     take(7, 1)
+    hand_over(5)
+    select_block(7)
+    pass_on(4)
+    hand_over(6)
     load_g.wait()
     load_u.wait()
     load_d.wait()
     compute(0)
-    hand_over(5)
-    pass_on(4)
-    select_block(7)
-    hand_over(6)
     pass_on(5)
-    compute(1)
     hand_over(7)
     pass_on(6)
     pass_on(7)
-    reduce_first(0)
+    compute(1)
+    send_halves(1)
     compute(2)
+    send_halves(2)
+    compute(3)
+    send_halves(3)
     reduce_first(1)
-    compute(3)
-    reduce_second(0)
 
     @scoped
     def weight_tile(i, carry):
@@ -611,7 +648,7 @@
 
     def sz_copy(k):
         return remote(
-            szs.at[k],
+            szs.at[place_of(k)],
             smat.at[pl.ds(pl.multiple_of(z * NE, NE), NE)],
             sent.at[12],
             got.at[3],
@@ -638,15 +675,16 @@
     @scoped
     def scores_y():
         arrived(syr.at[pl.ds(0, NE - 1)], got.at[2])
-        for k in range(NK):
-            szs[k] = jnp.concatenate([syr[e, k : k + 1, :] for e in range(NE)], axis=0)
-            part = pcodes[1, k] * at_ranks(pcodes[0, k], szs[k])
+        for n in range(NK):
+            k = block_at(n)
+            szs[n] = jnp.concatenate([syr[e, n : n + 1, :] for e in range(NE)], axis=0)
+            part = pcodes[1, k] * at_ranks(pcodes[0, k], szs[n])
             means[0, pl.ds(z_of(k), 1), :] = jnp.sum(part, axis=0, keepdims=True)
         for k in range(1, NK):
             mean_copy(k).start()
         for k in range(1, NK):
             sz_copy(k).start()
-        smat[pl.ds(pl.multiple_of(z * NE, NE), NE), :] = szs[0]
+        smat[pl.ds(pl.multiple_of(z * NE, NE), NE), :] = szs[place_of(0)]
 
     def dy_copy(d):
         j = (yc + d) % NE
@@ -699,33 +737,36 @@
             wide = jnp.where(mask, jnp.broadcast_to(rows[:, None, :], shape), 0.0)
             return jnp.sum(wide, axis=2, keepdims=True)
 
-        for k in range(NK):
-            mean = jnp.concatenate([de[j, pl.ds(z_of(k), 1), :] for j in range(NE)], axis=0)
-            code, gate = codes[0, k], codes[1, k]
+        for n in range(NK):
+            mean = jnp.concatenate([de[j, pl.ds(z_of(block_at(n)), 1), :] for j in range(NE)], axis=0)
+            code, gate = codes[0, n], codes[1, n]
             mine = jnp.broadcast_to(code[:, None, :], shape) == want
-            score = of_slots(lane == sub, sx[1, k * NE : (k + 1) * NE, :])
+            score = of_slots(lane == sub, sx[1, n * NE : (n + 1) * NE, :])
             slot_d = of_slots(mine, gate) * (score - of_slots(mine, mean))
-            rows = buf[0, k * NE : (k + 1) * NE, :, x_rows].astype(F32)
+            rows = buf[0, n * NE : (n + 1) * NE, :, x_rows].astype(F32)
             sums = sums + jnp.sum(slot_d * rows, axis=0)
         rg_ref[...] = jnp.sum(sums, axis=0, keepdims=True)
 
+    weight_tiles(0, 2)
+    reduce_first(2)
+    send_halves(0)
+    scores_x()
+    reduce_first(3)
     reduce_second(1)
-    reduce_first(2)
-    weight_tiles(0, 1)
-    scores_x()
-    combine(0)
-    weight_tiles(1, 2)
-    reduce_first(3)
-    combine(1)
+    weight_tiles(2, 3)
     reduce_second(2)
     scores_y()
-    weight_tiles(2, 3)
+    combine(1)
+    weight_tiles(3, 4)
+    reduce_first(0)
     reduce_second(3)
     combine(2)
-    weight_tiles(3, 5)
+    weight_tiles(4, 6)
+    reduce_second(0)
+    scores_z()
     combine(3)
-    scores_z()
-    weight_tiles(5, 8)
+    weight_tiles(6, 8)
+    combine(0)
     home_logits()
     router_out()
     token_out()
@@ -737,8 +778,8 @@
                 zbuf.at[seven],
                 tiles.at[seven],
                 etiles.at[seven, pl.ds(0, 64)],
-                ysend.at[pl.ds(0, 4)],
-                ysend.at[pl.ds(0, 5)],
+                buf.at[0, pl.ds(0, 4 * (NK - len(DIRECT)))],
+                buf.at[0, pl.ds(0, 5 * NK + 2 * len(DIRECT))],
                 buf.at[0],
                 sx.at[pl.ds(0, 3)],
                 r1,

time: 82.6 us -> 80.5 us (0.975)
  Pallas kernels: 81.1 us -> 79.6 us
    pallas_call x1, Pallas kernels: 78.9 us -> 77.4 us  [per_device(): pl.pallas_call(step_kernel, name='moe_backward', out_shape=shapes, in_spe...]
where the time goes in v3:
time: 80.5 us; the launch traced here: 80.4 us
  Pallas kernels  79.6 us (99%)
    pallas_call x1, Pallas kernels, per_device(): pl.pallas_call(step_kernel, name='moe_backward', out_shape=shapes, in_spe...  77.4 us
    pallas_call x1, Pallas kernels, per_device(): pl.pallas_call(finish_kernel, name='finish', out_shape=shapes, in_specs=[...  2.23 us

profile of v3, /device:TPU:1, one launch (start us, length us, event | category | flops | bytes accessed | tf_op | source)
XLA Modules:
  0.0 80.4 jit_solution(2903139084660272348)
XLA Ops:
  0.6 77.4 %moe_backward.1 = (bf16[48,512]{1,0:T(8,128)(2,1)S(1)}, f32[1,512]{1,0:T(1,128)S(1)}, bf16[2048,384]{1,0:T(8,128)(2,1)S(1)}, bf16[2048,384]{1,0:T(8,128)(2,1)S(1)}, bf16[384,2048]{1,0:T(8,128)(2,1)S(1)}) custom-call(bf16[48,2048]{1,0:T(8,128)(2,1)} %tok_hbm.1, bf16[48,2048]{1,0:T(8,128)(2,1)} %grad_hbm.1, s32[4,48]{1,0:T(4,128)} %bitcast.13, ...), custom_call_target="tpu_custom_call" | custom-call | tf_op jit(solution)/shard_map/moe_backward/pallas_call | solution.py:875
  78.0 2.2 %finish.1 = (bf16[48,512]{1,0:T(8,128)(2,1)}, f32[1,512]{1,0:T(1,128)}, bf16[2048,384]{1,0:T(8,128)(2,1)}, bf16[2048,384]{1,0:T(8,128)(2,1)}, bf16[384,2048]{1,0:T(8,128)(2,1)}) custom-call(bf16[48,512]{1,0:T(8,128)(2,1)S(1)} %get-tuple-element.15.tg, f32[1,512]{1,0:T(1,128)S(1)} %get-tuple-element.16.rg, bf16[2048,384]{1,0:T(8,128)(2,1)S(1)} %get-tuple-element.17.gg, ...), custom_call_target="tpu_custom_call" | custom-call | tf_op jit(solution)/shard_map/finish/pallas_call | solution.py:899

commit v4 on v3

--- a/solution.py
+++ b/solution.py
@@ -15,6 +15,8 @@
 CAP = 8
 PAIR_OF = (0, 2, 1, 4, 3, 6, 5, 7)
 GROUPS = ((0, 2), (2, 2), (4, 2), (6, 2))
+SUMMED = (None, (2, 2), (4, 2), (6, 1))
+WIDE = (1, 2, 0)
 DIRECT = (1, 2)
 
 
@@ -85,6 +87,11 @@
     r2,
     yret,
     yrr,
+    wide,
+    hzs,
+    hzr,
+    hxs,
+    hxr,
     wsend,
     wrecv,
     sx,
@@ -108,6 +115,7 @@
     r1r,
     r2r,
     vrs,
+    wyr,
 ):
     ep = lax.axis_index("ep")
     x = lax.axis_index("tp")
@@ -422,8 +430,8 @@
         return remote(sx.at[0, rows], sx.at[4 - d, rows], sent.at[6], got.at[0], ep, t)
 
     def unit(m, which):
-        k, n = GROUPS[m]
-        return pl.ds(k * NE + which * n * NE // 2, n * NE // 2)
+        n, count = SUMMED[m]
+        return pl.ds(n * NE + which * count * NE // 2, count * NE // 2)
 
     def halves_copy(m, which, slot):
         peer = near_b if which else near_a
@@ -434,8 +442,8 @@
         )
 
     def group(m):
-        k, n = GROUPS[m]
-        return pl.ds(k * NE, n * NE)
+        n, count = SUMMED[m]
+        return pl.ds(n * NE, count * NE)
 
     @scoped
     def compute(m):
@@ -524,12 +532,12 @@
 
     def back_copy(m, d):
         j = (yc + d) % NE
-        ks = pl.ds(*GROUPS[m])
+        ks = pl.ds(*SUMMED[m])
         return remote(yret.at[j, ks], yrr.at[yc, ks], sent.at[9], vrs.at[m], at_e(j), x)
 
     @scoped
     def reduce_second(m):
-        first, count = GROUPS[m]
+        first, count = SUMMED[m]
         wait_quarter(m)
         for k in range(first, first + count):
             rows = pl.ds(k * NE, NE)
@@ -548,18 +556,50 @@
 
     @scoped
     def back_waits(m):
-        arrived(yrr.at[pl.ds(0, NE - 1), pl.ds(*GROUPS[m])], vrs.at[m])
+        arrived(yrr.at[pl.ds(0, NE - 1), pl.ds(*SUMMED[m])], vrs.at[m])
 
     @scoped
     def combine(m):
         back_waits(m)
-        first, count = GROUPS[m]
+        first, count = SUMMED[m]
         for n in range(first, first + count):
             k = block_at(n)
             rows = jnp.concatenate([yrr[j, n] for j in range(NE)], axis=0)
             wsend[k] = dot_first(pbuf[k][:, 0:n_tok], rows).astype(BF16)
-            if k > 0:
-                home_copy(k).start()
+            home_copy(k).start()
+
+    @scoped
+    def wide_send(w):
+        n = place_of(WIDE[w])
+        for d in (1, 7, 2, 6, 3, 5, 4):
+            j = (yc + d) % NE
+            remote(
+                dxq.at[:, n * NE + j], wide.at[w, yc], sent.at[15], wyr.at[w], at_e(j), x
+            ).start()
+        wide[w, yc] = dxq[:, n * NE + yc]
+
+    @scoped
+    def wide_combine(w):
+        arrived(wide.at[w, pl.ds(0, NE - 1)], wyr.at[w])
+        k = WIDE[w]
+        place = pbuf[k][:, 0:n_tok]
+        for q in range(4):
+            rows = jnp.concatenate([wide[w, j, q] for j in range(NE)], axis=0)
+            hzs[w, q] = dot_first(place, rows).astype(BF16)
+        if k:
+            remote(
+                hzs.at[w], hzr.at[PAIR_OF[k] - 1], sent.at[16], got.at[6], at_z(z_of(k)), x
+            ).start()
+
+    @scoped
+    def wide_home():
+        arrived(hzr, got.at[6])
+        hxs[...] = (
+            hzs[2].astype(F32) + hzr[0].astype(F32) + hzr[1].astype(F32)
+        ).astype(BF16)
+        for d in (1, 3, 2):
+            t = (x + d) % 4
+            remote(hxs.at[t], hxr.at[3 - d], sent.at[17], got.at[7], ep, t).start()
 
     def both(f, *ks):
         for k in ks:
@@ -606,6 +646,8 @@
     compute(0)
     pass_on(5)
     hand_over(7)
+    wide_send(0)
+    wide_send(1)
     pass_on(6)
     pass_on(7)
     compute(1)
@@ -614,6 +656,7 @@
     send_halves(2)
     compute(3)
     send_halves(3)
+    wide_send(2)
     reduce_first(1)
 
     @scoped
@@ -718,9 +761,12 @@
         d_lo = (d_t - d_hi.astype(F32)).astype(BF16)
         rw_x = rwv[:, x_rows]
         total = (dot_first(d_hi, rw_x) + dot_first(d_lo, rw_x))[0:n_tok, :]
-        total = total + wsend[0].astype(F32)
-        arrived(wrecv.at[pl.ds(1, NK - 1)], got.at[1])
-        for k in range(1, NK):
+        arrived(hxr, got.at[7])
+        total = total + hxs[x].astype(F32)
+        for d in range(3):
+            total = total + hxr[d].astype(F32)
+        arrived(wrecv.at[pl.ds(3, NK - 3)], got.at[1])
+        for k in range(3, NK):
             total = total + wrecv[k].astype(F32)
         tg_ref[...] = total.astype(BF16)
 
@@ -747,26 +793,25 @@
             sums = sums + jnp.sum(slot_d * rows, axis=0)
         rg_ref[...] = jnp.sum(sums, axis=0, keepdims=True)
 
-    weight_tiles(0, 2)
+    wide_combine(0)
+    wide_combine(1)
     reduce_first(2)
-    send_halves(0)
     scores_x()
+    weight_tiles(0, 1)
     reduce_first(3)
     reduce_second(1)
-    weight_tiles(2, 3)
+    weight_tiles(1, 2)
     reduce_second(2)
     scores_y()
+    wide_combine(2)
+    wide_home()
+    reduce_second(3)
     combine(1)
-    weight_tiles(3, 4)
-    reduce_first(0)
-    reduce_second(3)
+    weight_tiles(2, 4)
     combine(2)
-    weight_tiles(4, 6)
-    reduce_second(0)
+    combine(3)
     scores_z()
-    combine(3)
-    weight_tiles(6, 8)
-    combine(0)
+    weight_tiles(4, 8)
     home_logits()
     router_out()
     token_out()
@@ -782,14 +827,17 @@
                 buf.at[0, pl.ds(0, 5 * NK + 2 * len(DIRECT))],
                 buf.at[0],
                 sx.at[pl.ds(0, 3)],
-                r1,
-                s2,
-                yret.at[seven],
-                wsend.at[seven],
+                r1.at[:, pl.ds(0, 5 * NE)],
+                s2.at[pl.ds(0, 5 * NE)],
+                yret.at[seven, pl.ds(0, 5)],
+                wsend.at[pl.ds(0, 5)],
                 sy.at[seven],
                 szs.at[seven],
                 means.at[seven],
                 means.at[seven],
+                wide.at[:, seven],
+                hzr,
+                hxr,
             )
         ):
             arrived(ref, sent.at[i])
@@ -841,6 +889,11 @@
         pltpu.VMEM((slots, CAP, quarter), BF16),
         pltpu.VMEM((NE, NK, CAP, quarter), BF16),
         pltpu.VMEM((NE, NK, CAP, quarter), BF16),
+        pltpu.VMEM((3, NE, 4, CAP, quarter), BF16),
+        pltpu.VMEM((3, 4, n_tok, quarter), BF16),
+        pltpu.VMEM((2, 4, n_tok, quarter), BF16),
+        pltpu.VMEM((4, n_tok, quarter), BF16),
+        pltpu.VMEM((3, n_tok, quarter), BF16),
         pltpu.VMEM((NK, n_tok, quarter), BF16),
         pltpu.VMEM((NK, n_tok, quarter), BF16),
         pltpu.VMEM((4, slots, 128), F32),
@@ -853,8 +906,8 @@
         pltpu.VMEM((NK, 128), F32),
         pltpu.VMEM((NE, NK, 128), F32),
         dma((7,)),
-        dma((15,)),
-        dma((6,)),
+        dma((18,)),
+        dma((8,)),
         dma((8, 2)),
         dma((8,)),
         dma((8,)),
@@ -864,6 +917,7 @@
         dma((4, 2)),
         dma((4,)),
         dma((4,)),
+        dma((3,)),
     ]
     shapes = (
         jax.ShapeDtypeStruct((n_tok, quarter), BF16),

time: 80.5 us -> 77.4 us (0.961)
  Pallas kernels: 79.6 us -> 76.4 us
    pallas_call x1, Pallas kernels: 77.4 us -> 74.1 us  [per_device(): pl.pallas_call(step_kernel, name='moe_backward', out_shape=shapes, in_spe...]
where the time goes in v4:
time: 77.4 us; the launch traced here: 77 us
  Pallas kernels  76.4 us (99%)
    pallas_call x1, Pallas kernels, per_device(): pl.pallas_call(step_kernel, name='moe_backward', out_shape=shapes, in_spe...  74.1 us
    pallas_call x1, Pallas kernels, per_device(): pl.pallas_call(finish_kernel, name='finish', out_shape=shapes, in_specs=[...  2.23 us

profile of v4, /device:TPU:1, one launch (start us, length us, event | category | flops | bytes accessed | tf_op | source)
XLA Modules:
  0.0 77.0 jit_solution(12740417082915800813)
XLA Ops:
  0.6 74.1 %moe_backward.1 = (bf16[48,512]{1,0:T(8,128)(2,1)S(1)}, f32[1,512]{1,0:T(1,128)S(1)}, bf16[2048,384]{1,0:T(8,128)(2,1)S(1)}, bf16[2048,384]{1,0:T(8,128)(2,1)S(1)}, bf16[384,2048]{1,0:T(8,128)(2,1)S(1)}) custom-call(bf16[48,2048]{1,0:T(8,128)(2,1)} %tok_hbm.1, bf16[48,2048]{1,0:T(8,128)(2,1)} %grad_hbm.1, s32[4,48]{1,0:T(4,128)} %bitcast.13, ...), custom_call_target="tpu_custom_call" | custom-call | tf_op jit(solution)/shard_map/moe_backward/pallas_call | solution.py:929
  74.8 2.2 %finish.1 = (bf16[48,512]{1,0:T(8,128)(2,1)}, f32[1,512]{1,0:T(1,128)}, bf16[2048,384]{1,0:T(8,128)(2,1)}, bf16[2048,384]{1,0:T(8,128)(2,1)}, bf16[384,2048]{1,0:T(8,128)(2,1)}) custom-call(bf16[48,512]{1,0:T(8,128)(2,1)S(1)} %get-tuple-element.15.tg, f32[1,512]{1,0:T(1,128)S(1)} %get-tuple-element.16.rg, bf16[2048,384]{1,0:T(8,128)(2,1)S(1)} %get-tuple-element.17.gg, ...), custom_call_target="tpu_custom_call" | custom-call | tf_op jit(solution)/shard_map/finish/pallas_call | solution.py:953

commit v5 on v4

--- a/solution.py
+++ b/solution.py
@@ -68,6 +68,9 @@
     wg,
     wu,
     wd,
+    wgt,
+    wut,
+    wdt,
     zbuf,
     tiles,
     etiles,
@@ -446,6 +449,18 @@
         return pl.ds(n * NE, count * NE)
 
     @scoped
+    def turn_down():
+        load_d.wait()
+        for i in range(0, 2048, 256):
+            wdt[i : i + 256, :] = wd[:, i : i + 256].T
+
+    @scoped
+    def turn(load, w, wt):
+        load.wait()
+        for i in range(0, 2048, 256):
+            wt[:, i : i + 256] = w[i : i + 256, :].T
+
+    @scoped
     def compute(m):
         first, count = GROUPS[m]
         n_rows = count * NE * CAP
@@ -469,7 +484,7 @@
         gin = buf[1, rows].reshape(n_rows, 2048)
         gate_pre = dot(xin, wg[...])
         up_pre = dot(xin, wu[...])
-        back = dot_last(gin, wd[...])
+        back = dot(gin, wdt[...])
         glu = jnp.minimum(gate_pre, 7.0)
         lin1 = jnp.clip(up_pre, -7.0, 7.0) + 1.0
         sig = jax.nn.sigmoid(1.702 * glu)
@@ -494,7 +509,7 @@
 
         for q in range(4):
             cols = slice(512 * q, 512 * (q + 1))
-            part = dot_last(d_gate, wg[cols, :]) + dot_last(d_up, wu[cols, :])
+            part = dot(d_gate, wgt[:, cols]) + dot(d_up, wut[:, cols])
             dxq[q, rows] = part.astype(BF16).reshape(count * NE, CAP, 512)
     @scoped
     def send_halves(m):
@@ -624,6 +639,7 @@
     pass_on(0)
     takes(1, 3, 4)
     select_block(3)
+    turn_down()
     pass_on(1)
     select_block(4)
     pass_on(2)
@@ -632,6 +648,7 @@
     hand_over(4)
     takes(1, 5, 6)
     select_block(5)
+    turn(load_g, wg, wgt)
     pass_on(3)
     select_block(6)
     take(7, 0)
@@ -639,10 +656,8 @@
     hand_over(5)
     select_block(7)
     pass_on(4)
+    turn(load_u, wu, wut)
     hand_over(6)
-    load_g.wait()
-    load_u.wait()
-    load_d.wait()
     compute(0)
     pass_on(5)
     hand_over(7)
@@ -870,6 +885,9 @@
         pltpu.VMEM((width, ff), BF16),
         pltpu.VMEM((width, ff), BF16),
         pltpu.VMEM((ff, width), BF16),
+        pltpu.VMEM((ff, width), BF16),
+        pltpu.VMEM((ff, width), BF16),
+        pltpu.VMEM((width, ff), BF16),
         pltpu.VMEM((NK, n_tok, width), BF16),
         pltpu.VMEM((NK, 8, 128), F32),
         pltpu.VMEM((NK, NE * 8, 128), F32),

time: 77.4 us -> 77.8 us (level)
  no operation moved by 1% of the time
where the time goes in v5:
time: 77.8 us
  Pallas kernels  77.1 us (99%)
    pallas_call x1, Pallas kernels, per_device(): pl.pallas_call(step_kernel, name='moe_backward', out_shape=shapes, in_spe...  74.9 us
    pallas_call x1, Pallas kernels, per_device(): pl.pallas_call(finish_kernel, name='finish', out_shape=shapes, in_specs=[...  2.23 us

profile of v5, /device:TPU:1, one launch (start us, length us, event | category | flops | bytes accessed | tf_op | source)
XLA Modules:
  0.0 77.8 jit_solution(11805528507071444702)
XLA Ops:
  0.6 74.9 %moe_backward.1 = (bf16[48,512]{1,0:T(8,128)(2,1)S(1)}, f32[1,512]{1,0:T(1,128)S(1)}, bf16[2048,384]{1,0:T(8,128)(2,1)S(1)}, bf16[2048,384]{1,0:T(8,128)(2,1)S(1)}, bf16[384,2048]{1,0:T(8,128)(2,1)S(1)}) custom-call(bf16[48,2048]{1,0:T(8,128)(2,1)} %tok_hbm.1, bf16[48,2048]{1,0:T(8,128)(2,1)} %grad_hbm.1, s32[4,48]{1,0:T(4,128)} %bitcast.13, ...), custom_call_target="tpu_custom_call" | custom-call | tf_op jit(solution)/shard_map/moe_backward/pallas_call | solution.py:947
  75.5 2.2 %finish.1 = (bf16[48,512]{1,0:T(8,128)(2,1)}, f32[1,512]{1,0:T(1,128)}, bf16[2048,384]{1,0:T(8,128)(2,1)}, bf16[2048,384]{1,0:T(8,128)(2,1)}, bf16[384,2048]{1,0:T(8,128)(2,1)}) custom-call(bf16[48,512]{1,0:T(8,128)(2,1)S(1)} %get-tuple-element.15.tg, f32[1,512]{1,0:T(1,128)S(1)} %get-tuple-element.16.rg, bf16[2048,384]{1,0:T(8,128)(2,1)S(1)} %get-tuple-element.17.gg, ...), custom_call_target="tpu_custom_call" | custom-call | tf_op jit(solution)/shard_map/finish/pallas_call | solution.py:971
